TPU v7x, 32 devices: a whole 2x2x4 slice. The times are simulated.
32 devices in a mesh: sp: 8 (over z, core), tp: 4 (over y, x).
Axes of the slice: x: 2, y: 2, z: 4, core: 2. Of those that a mesh axis runs over, the one named last changes fastest.
Arguments:
- queries: bfloat16 [2048, 2048], P('sp', 'tp'), may hold values from -8 to 8
- key_rows: bfloat16 [2048, 1024], P('sp', 'tp'), may hold values from -8 to 8
- values: bfloat16 [2048, 1024], P('sp', 'tp'), may hold values from -6 to 6
- sink_logits: float32 [32], P('tp'), may hold values from 2 to 6
- residual: bfloat16 [2048, 2048], P(('sp', 'tp')), may hold values from -6 to 6
- out_weight: bfloat16 [2048, 2048], P('tp'), may hold values from -0.125 to 0.125
- norm_gain: float32 [2048], replicated, may hold values from 0.1 to 1.9
- expert_ids: int32 [2048, 2], P('sp'), may hold values from 0 to 7, as said below
- route_weight: float32 [2048, 2], P('sp'), may hold values from 0.2 to 1
- gate_proj: bfloat16 [8, 2048, 4096], P('sp', None, 'tp'), may hold values from -0.125 to 0.125
- up_proj: bfloat16 [8, 2048, 4096], P('sp', None, 'tp'), may hold values from -0.125 to 0.125
- down_proj: bfloat16 [8, 4096, 2048], P('sp', 'tp'), may hold values from -0.09375 to 0.09375
Outputs:
- mixed_out: bfloat16 [2048, 2048], P(('sp', 'tp'))
Inputs may be any that keep to these rules, and one draw needn't show every extreme that they name: `expert_ids`: the two entries of a row are different experts of one group: experts g * 2 to g * 2 + 1 for a group g below 4. In each aligned block of 64 rows (the rows of one device) no expert is named more than 32 times, and one expert is named exactly 32 times in every block.
All inputs are finite; a program needn't handle non-finite values.
Results may differ from a plain program's by a relative error of at most 0.014.
Values may be sent and summed in bfloat16 or wider, within the bound.
A program may use at most 64 MiB of HBM per device.

v0:
```python
import jax
import jax.numpy as jnp
from jax import lax
from jax.experimental import pallas as pl
from jax.experimental.pallas import tpu as pltpu
from jax.sharding import PartitionSpec as P

HEAD = 64
WINDOW = 128


norm_epsilon = 1e-06


def from_behind(block, axis, distance):
    devices = range(lax.axis_size(axis))
    route = [(i - distance, i) for i in devices if i - distance in devices]
    return lax.ppermute(block, axis, route)


def rotary(values_in, positions, head_count):
    halfway = HEAD // 2
    frequency = 10000.0 ** (-jnp.arange(halfway, dtype=jnp.float32) * 2.0 / HEAD)
    angles = positions.astype(jnp.float32)[:, None] * frequency[None, :]
    cosine = jnp.cos(angles)[:, None, :]
    sine_part = jnp.sin(angles)[:, None, :]
    reshaped = values_in.astype(jnp.float32).reshape(values_in.shape[0], head_count, HEAD)
    front_part = reshaped[..., :halfway]
    back_part = reshaped[..., halfway:]
    turned = jnp.concatenate(
        [front_part * cosine - back_part * sine_part, back_part * cosine + front_part * sine_part],
        -1,
    )
    return turned.astype(jnp.bfloat16)


def attend(query_blocks, key_pairs, value_pairs, sink_grid, key_start):
    block_count = query_blocks.shape[0]
    window_len = query_blocks.shape[1]
    scores = jnp.einsum(
        "bqkgd,bskd->bkgqs", query_blocks, key_pairs, preferred_element_type=jnp.float32
    ) * HEAD ** (-0.5)
    row_idx = jnp.arange(window_len)[:, None]
    col_idx = jnp.arange(2 * window_len)[None, :]
    distance = row_idx - col_idx + window_len
    key_pos = key_start + jnp.arange(block_count)[:, None, None] * window_len + col_idx[None]
    allowed = (distance >= 0)[None] & (distance < window_len)[None] & (key_pos >= 0)
    scores = jnp.where(allowed[:, None, None], scores, -jnp.inf)
    sink_full = sink_grid[None, :, :, None]
    highest = jnp.maximum(jnp.max(scores, -1), sink_full)
    exp_scores = jnp.exp(scores - highest[..., None])
    denominator = jnp.sum(exp_scores, -1) + jnp.exp(sink_full - highest)
    weighted = jnp.einsum(
        "bkgqs,bskd->bkgqd",
        exp_scores.astype(jnp.bfloat16),
        value_pairs,
        preferred_element_type=jnp.float32,
    )
    normalized = weighted / denominator[..., None]
    return (
        jnp.transpose(normalized, (0, 3, 1, 2, 4))
        .astype(jnp.bfloat16)
        .reshape(block_count * window_len, -1)
    )


def slot_select(picks_in, expert_count, capacity):
    flattened = picks_in.reshape(-1)
    onehot = (flattened[:, None] == jnp.arange(expert_count, dtype=jnp.int32)[None, :]).astype(
        jnp.int32
    )
    rank_of = jnp.sum(jnp.cumsum(onehot, 0) * onehot, 1) - 1
    slot_of = flattened * capacity + rank_of
    chosen = jnp.arange(expert_count * capacity, dtype=jnp.int32)[:, None] == slot_of[None, :]
    return chosen.astype(jnp.bfloat16)


def expert_part(rows_in, gate_proj, up_proj, down_proj):
    in_shape = rows_in.shape
    flattened = rows_in.reshape(-1, in_shape[-1])
    gate_val = jnp.dot(flattened, gate_proj[0], preferred_element_type=jnp.float32)
    up_val = jnp.dot(flattened, up_proj[0], preferred_element_type=jnp.float32)
    hidden = (jax.nn.silu(gate_val) * up_val).astype(jnp.bfloat16)
    return (
        jnp.dot(hidden, down_proj[0], preferred_element_type=jnp.float32)
        .astype(jnp.bfloat16)
        .reshape(in_shape)
    )


GROUPS = 4
TILE = 256
MESH = pl.DeviceIdType.MESH


def group_kernel(
    proj, resid, gain, extra, sel, sel_back, wg_hbm, wu_hbm, wd_hbm, out,
    wg, wu, wd, w_sem,
    rs_in, rs_s, rs_r,
    mid, normed, outb, rows,
    di_s, di_r, ag_s, ag_r, pt_s, pt_r,
    hid, outp, pr, pr_s, pr_r,
    comb, rs2, r2_s, r2_r,
    ret, back, bk_s, bk_r,
):
    sp = lax.axis_index("sp")
    t = lax.axis_index("tp")
    core = lax.rem(sp, 2)
    z = sp // 2
    tp_n, row_n, width = proj.shape
    ext_width = normed.shape[1]
    cap = outb.shape[1]
    half = GROUPS * cap
    flip1 = t + 1 - 2 * lax.rem(t, 2)
    flip2 = lax.rem(t + 2, 4)
    flip3 = lax.rem(flip1 + 2, 4)
    peer = [t, flip1, flip2, flip3]
    partner = sp + 1 - 2 * core
    zoff = lambda k: lax.rem(z + k + GROUPS, GROUPS)

    loads = [
        pltpu.make_async_copy(a, b, w_sem.at[i])
        for i, (a, b) in enumerate(((wg_hbm, wg), (wu_hbm, wu), (wd_hbm, wd)))
    ]
    for c in loads:
        c.start()

    barrier = pltpu.get_barrier_semaphore()
    friends = [(sp, peer[d]) for d in (1, 2, 3)]
    friends += [(zoff(k) * 2 + core, t) for k in (1, 2, 3)] + [(partner, t)]
    for dev in friends:
        pl.semaphore_signal(barrier, inc=1, device_id=dev, device_id_type=MESH)
    pl.semaphore_wait(barrier, len(friends))

    sent = []

    def send(src, dst, ss, rs, dev):
        c = pltpu.make_async_remote_copy(
            src_ref=src, dst_ref=dst, send_sem=ss, recv_sem=rs, device_id=dev, device_id_type=MESH
        )
        c.start()
        sent.append(c)
        return c

    firsts = [
        send(proj.at[peer[d]], rs_in.at[d - 1], rs_s.at[d - 1], rs_r.at[d - 1], (sp, peer[d]))
        for d in (3, 1, 2)
    ]
    for c in firsts:
        c.wait_recv()
    total = resid[...].astype(jnp.float32) + (
        proj[t].astype(jnp.float32)
        + rs_in[0].astype(jnp.float32)
        + rs_in[1].astype(jnp.float32)
        + rs_in[2].astype(jnp.float32)
    )
    middle = total.astype(jnp.bfloat16)
    mid[...] = middle
    mf = middle.astype(jnp.float32)
    scale = lax.rsqrt(jnp.mean(mf * mf, -1, keepdims=True) + norm_epsilon)
    normed[:, :width] = (mf * scale * gain[...]).astype(jnp.bfloat16)
    normed[:, width:] = extra[...]

    def block(tt, cc, zz):
        return rows.at[zz, pl.ds(pl.multiple_of((cc * tp_n + tt) * cap, cap), cap)]

    def pack(g):
        s = sel[pl.ds(pl.multiple_of(g * cap, cap), cap), :]
        return jnp.dot(s, normed[...], preferred_element_type=jnp.float32).astype(jnp.bfloat16)

    order = (0, 1, 3, 2)
    ag = {}
    pt = {}

    def push(d, k, tt, to):
        ref = block(tt, core, zoff(-k))
        ag[(d, k)] = send(ref, ref, ag_s.at[d - 1, k], ag_r.at[d - 1, k], (sp, peer[to]))

    def across(d, k):
        ref = block(peer[d], core, zoff(-k))
        pt[(d, k)] = send(ref, ref, pt_s.at[d, k], pt_r.at[d, k], (partner, t))

    disp = [None] * GROUPS

    def spread(i):
        k = order[i]
        if k:
            disp[k].wait_recv()
        push(1, k, t, 1)
        push(2, k, t, 2)
        across(0, k)

    def relay(i):
        k = order[i]
        via = 1 + i % 2
        ag[(via, k)].wait_recv()
        push(3, k, peer[via], 3 - via)
        across(via, k)
        ag[(3 - via, k)].wait_recv()
        across(3 - via, k)

    def corner(i):
        k = order[i]
        ag[(3, k)].wait_recv()
        across(3, k)

    def widen(i):
        k = order[i]
        zz = zoff(-k)
        for d in (0, 1, 2, 3):
            pt[(d, k)].wait_recv()

        @pl.loop(0, wg.shape[1] // TILE)
        def _(n):
            cols = pl.ds(pl.multiple_of(n * TILE, TILE), TILE)
            x = rows[zz, :, :width]
            g = jnp.dot(x, wg[:, cols], preferred_element_type=jnp.float32)
            u = jnp.dot(x, wu[:, cols], preferred_element_type=jnp.float32)
            hid[:, cols] = (g / (1.0 + jnp.exp(-g)) * u).astype(jnp.bfloat16)

    swap = {}

    def narrow(i):
        k = order[i]
        ext = rows[zoff(-k), :, width:].astype(jnp.float32)
        lane = lax.broadcasted_iota(jnp.int32, ext.shape, 1)
        mine = (lane == core) | (lane == core + 2)
        weight = jnp.sum(jnp.where(mine, ext, 0.0), -1, keepdims=True)

        @pl.loop(0, width // TILE)
        def _(n):
            cols = pl.ds(pl.multiple_of(n * TILE, TILE), TILE)
            y = jnp.dot(hid[...], wd[:, cols], preferred_element_type=jnp.float32)
            outp[k, :, cols] = (y * weight).astype(jnp.bfloat16)

        other = outp.at[k, pl.ds(pl.multiple_of((1 - core) * half, half), half)]
        swap[k] = send(other, pr.at[k], pr_s.at[k], pr_r.at[k], (partner, t))

    def own(k, d):
        off = pl.multiple_of((core * tp_n + peer[d]) * cap, cap)
        here = pl.ds(pl.multiple_of(peer[d] * cap, cap), cap)
        return outp[k, pl.ds(off, cap), :].astype(jnp.float32) + pr[k, here, :].astype(jnp.float32)

    r2 = {}

    def ship(k, d, to):
        r2[(d, k)] = send(
            comb.at[k, d - 1], rs2.at[k, d - 1],
            r2_s.at[d - 1, k], r2_r.at[d - 1, k], (sp, peer[to]),
        )

    def combine(i):
        k = order[i]
        via = 1 + i % 2
        swap[k].wait_recv()
        comb[k, 2] = own(k, 3).astype(jnp.bfloat16)
        ship(k, 3, via)
        comb[k, via - 1] = own(k, via).astype(jnp.bfloat16)
        ship(k, via, via)

    def combine_on(i):
        k = order[i]
        on = 2 - i % 2
        r2[(3, k)].wait_recv()
        comb[k, on - 1] = (own(k, on) + rs2[k, 2].astype(jnp.float32)).astype(jnp.bfloat16)
        ship(k, on, on)

    bk = []

    def finish(i):
        k = order[i]
        acc = own(k, 0)
        for d in (1, 2):
            r2[(d, k)].wait_recv()
            acc = acc + rs2[k, d - 1].astype(jnp.float32)
        if k:
            ret[k] = acc.astype(jnp.bfloat16)
            bk.append(
                send(
                    ret.at[k], back.at[z], bk_s.at[k - 1], bk_r.at[k - 1],
                    (2 * zoff(-k) + core, t),
                )
            )
        else:
            back[z] = acc.astype(jnp.bfloat16)

    block(t, core, z)[...] = pack(z)
    spread(0)
    for k in (1, 3, 2):
        g = zoff(k)
        outb[k] = pack(g)
        disp[k] = send(
            outb.at[k], block(t, core, z), di_s.at[k - 1], di_r.at[k - 1], (2 * g + core, t)
        )
    relay(0)
    corner(0)
    spread(1)
    for c in loads:
        c.wait()
    widen(0)
    relay(1)
    spread(2)
    narrow(0)
    corner(1)
    widen(1)
    relay(2)
    spread(3)
    combine(0)
    narrow(1)
    corner(2)
    widen(2)
    relay(3)
    combine_on(0)
    combine(1)
    narrow(2)
    corner(3)
    combine_on(1)
    widen(3)
    finish(0)
    combine(2)
    narrow(3)
    finish(1)
    combine_on(2)
    combine(3)
    finish(2)
    combine_on(3)
    finish(3)
    for c in bk:
        c.wait_recv()
    routed = jnp.dot(
        sel_back[...], back[...].reshape(half, width), preferred_element_type=jnp.float32
    )
    out[...] = (mid[...].astype(jnp.float32) + routed).astype(jnp.bfloat16)
    for c in sent:
        c.wait_send()


def group_experts(projected, residual, norm_gain, own_ids, own_weights, gate, up, down):
    row_n, width = residual.shape
    tp_n = lax.axis_size("tp")
    expert_n = lax.axis_size("sp")
    cap = 2 * max(1, 2 * row_n // expert_n)
    group = own_ids[:, 0] // 2
    onehot = (group[:, None] == jnp.arange(GROUPS, dtype=jnp.int32)[None, :]).astype(jnp.int32)
    rank_of = jnp.sum(jnp.cumsum(onehot, 0) * onehot, 1) - 1
    slot = group * cap + rank_of
    hit = jnp.arange(GROUPS * cap, dtype=jnp.int32)[:, None] == slot[None, :]
    sel = hit.astype(jnp.bfloat16)
    odd = lax.rem(own_ids, 2)
    pair = jnp.stack(
        [jnp.sum(jnp.where(odd == p, own_weights, 0.0), 1) for p in (0, 1)], 1
    )
    high = pair.astype(jnp.bfloat16)
    low = (pair - high.astype(jnp.float32)).astype(jnp.bfloat16)
    extra = jnp.pad(jnp.concatenate([high, low], 1), ((0, 0), (0, 124)))
    ext_width = width + 128
    ff = gate.shape[-1]
    half = GROUPS * cap
    bf = jnp.bfloat16
    dma = pltpu.SemaphoreType.DMA
    vmem = pl.BlockSpec(memory_space=pltpu.VMEM)
    hbm = pl.BlockSpec(memory_space=pl.ANY)
    return pl.pallas_call(
        group_kernel,
        out_shape=jax.ShapeDtypeStruct((row_n, width), bf),
        in_specs=[vmem] * 6 + [hbm] * 3,
        out_specs=vmem,
        scratch_shapes=[
            pltpu.VMEM((width, ff), bf),
            pltpu.VMEM((width, ff), bf),
            pltpu.VMEM((ff, width), bf),
            dma((3,)),
            pltpu.VMEM((3, row_n, width), bf),
            dma((3,)),
            dma((3,)),
            pltpu.VMEM((row_n, width), bf),
            pltpu.VMEM((row_n, ext_width), bf),
            pltpu.VMEM((GROUPS, cap, ext_width), bf),
            pltpu.VMEM((GROUPS, 2 * half, ext_width), bf),
            dma((3,)),
            dma((3,)),
            dma((3, GROUPS)),
            dma((3, GROUPS)),
            dma((4, GROUPS)),
            dma((4, GROUPS)),
            pltpu.VMEM((2 * half, ff), bf),
            pltpu.VMEM((4, 2 * half, width), bf),
            pltpu.VMEM((4, half, width), bf),
            dma((4,)),
            dma((4,)),
            pltpu.VMEM((GROUPS, 3, cap, width), bf),
            pltpu.VMEM((GROUPS, 3, cap, width), bf),
            dma((3, GROUPS)),
            dma((3, GROUPS)),
            pltpu.VMEM((GROUPS, cap, width), bf),
            pltpu.VMEM((GROUPS, cap, width), bf),
            dma((3,)),
            dma((3,)),
        ],
        compiler_params=pltpu.CompilerParams(
            collective_id=0, has_side_effects=True, vmem_limit_bytes=56 * 2**20
        ),
    )(
        projected.reshape(tp_n, row_n, width), residual, norm_gain[None], extra, sel,
        sel.T, gate[0], up[0], down[0],
    )


def per_device(
    queries,
    key_rows,
    values,
    sink_logits,
    residual,
    out_weight,
    norm_gain,
    expert_ids,
    route_weight,
    gate_proj,
    up_proj,
    down_proj,
):
    local_len = queries.shape[0]
    q_heads = sink_logits.shape[0]
    kv_heads = key_rows.shape[1] // HEAD
    group_size = q_heads // kv_heads
    window_len = WINDOW
    seq_start = lax.axis_index("sp") * local_len
    rim_pair = jnp.stack([key_rows[local_len - window_len :], values[local_len - window_len :]])
    rim_pair = from_behind(rim_pair, "sp", 1)
    key_ext = jnp.concatenate([rim_pair[0], key_rows], 0)
    val_ext = jnp.concatenate([rim_pair[1], values], 0)
    positions = seq_start + jnp.arange(local_len, dtype=jnp.int32)
    ext_positions = seq_start - window_len + jnp.arange(local_len + window_len, dtype=jnp.int32)
    rot_query = rotary(queries, positions, q_heads)
    rot_key = rotary(key_ext, ext_positions, kv_heads)
    block_count = local_len // window_len
    query_blocks = rot_query.reshape(block_count, window_len, kv_heads, group_size, HEAD)
    key_blocks = rot_key.reshape(block_count + 1, window_len, kv_heads, HEAD)
    value_blocks = val_ext.reshape(block_count + 1, window_len, kv_heads, HEAD)
    key_pairs = jnp.concatenate([key_blocks[:-1], key_blocks[1:]], 1)
    value_pairs = jnp.concatenate([value_blocks[:-1], value_blocks[1:]], 1)
    sink_grid = sink_logits.reshape(kv_heads, group_size)
    attended = attend(query_blocks, key_pairs, value_pairs, sink_grid, seq_start - window_len)
    tok_rows = residual.shape[0]
    tp_count = lax.axis_size("tp")
    tp_index = lax.axis_index("tp")
    if tp_count == 4 and lax.axis_size("sp") == 2 * GROUPS:
        return group_experts(
            jnp.dot(attended, out_weight, preferred_element_type=jnp.float32).astype(
                jnp.bfloat16
            ),
            residual,
            norm_gain,
            lax.dynamic_slice_in_dim(expert_ids, tp_index * tok_rows, tok_rows, 0),
            lax.dynamic_slice_in_dim(route_weight, tp_index * tok_rows, tok_rows, 0),
            gate_proj,
            up_proj,
            down_proj,
        )
    projected = lax.psum_scatter(
        jnp.dot(attended, out_weight, preferred_element_type=jnp.float32).astype(jnp.bfloat16),
        "tp",
        scatter_dimension=0,
        tiled=True,
    ).astype(jnp.float32)
    middle = (residual.astype(jnp.float32) + projected).astype(jnp.bfloat16)
    middle_f = middle.astype(jnp.float32)
    normed = (
        middle_f
        * lax.rsqrt(jnp.mean(middle_f * middle_f, -1, keepdims=True) + norm_epsilon)
        * norm_gain
    ).astype(jnp.bfloat16)
    expert_count = lax.axis_size("sp")
    capacity = 2 * max(1, 2 * tok_rows // expert_count)
    model_width = normed.shape[1]
    own_ids = lax.dynamic_slice_in_dim(expert_ids, tp_index * tok_rows, tok_rows, 0)
    own_weights = lax.dynamic_slice_in_dim(route_weight, tp_index * tok_rows, tok_rows, 0)
    select = slot_select(own_ids, expert_count, capacity)
    token_select = jnp.sum(select.reshape(expert_count * capacity, tok_rows, 2), -1)
    outbound = jnp.dot(token_select, normed, preferred_element_type=jnp.float32).astype(
        jnp.bfloat16
    )
    outbound = outbound.reshape(expert_count, capacity, model_width)
    arrived = lax.all_to_all(outbound, "sp", split_axis=0, concat_axis=0, tiled=True)
    partial_out = expert_part(
        lax.all_gather(arrived, "tp", axis=0, tiled=True), gate_proj, up_proj, down_proj
    )
    partial_out = partial_out.reshape(tp_count, expert_count * capacity, model_width)
    width_parts = lax.all_to_all(partial_out, "tp", split_axis=0, concat_axis=0, tiled=True)
    summed = jnp.sum(width_parts.astype(jnp.float32), 0).reshape(
        expert_count, capacity, model_width
    )
    returned = (
        lax.all_to_all(summed.astype(jnp.bfloat16), "sp", split_axis=0, concat_axis=0, tiled=True)
        .astype(summed.dtype)
        .reshape(expert_count * capacity, model_width)
    )
    picked = jnp.dot(
        select.astype(jnp.float32).T,
        returned,
        precision=lax.Precision.HIGHEST,
        preferred_element_type=jnp.float32,
    )
    routed = jnp.sum(picked.reshape(tok_rows, 2, model_width) * own_weights[..., None], 1)
    return (middle_f + routed).astype(jnp.bfloat16)


def solution(mesh):
    return jax.shard_map(
        per_device,
        mesh=mesh,
        in_specs=(
            P("sp", "tp"),
            P("sp", "tp"),
            P("sp", "tp"),
            P("tp"),
            P(("sp", "tp"), None),
            P("tp", None),
            P(),
            P("sp", None),
            P("sp", None),
            P("sp", None, "tp"),
            P("sp", None, "tp"),
            P("sp", "tp", None),
        ),
        out_specs=P(("sp", "tp"), None),
        check_vma=False,
    )
```

profile of v0, /device:TPU:0, one launch (start us, length us, event | category | flops | bytes accessed | tf_op | source)
XLA Modules:
  0.0 108.3 jit_solution(1445413925044406356)
XLA Ops:
  0.0 0.0 copy-start
  0.0 1.1 %copy.33 = bf16[256,256]{0,1:T(8,128)(2,1)S(1)} copy(bf16[256,256]{1,0:T(8,128)(2,1)} %param.13) | data formatting | bytes 262144 | tf_op args[1]
  1.2 0.8 slice.50
  2.0 0.1 copy.56
  2.1 0.0 copy-start.3
  2.2 2.4 %collective-permute-start = (bf16[2,128,256]{1,2,0:T(8,128)(2,1)S(1)}, bf16[2,128,256]{1,2,0:T(8,128)(2,1)S(1)}, u32[]{:S(2)}, u32[]{:S(2)}) collective-permute-start(bf16[2,128,256]{1,2,0:T(8,128)(2,1)S(1)} %pad_maximum_fusion.2), channel_id=1, source_target_pairs={{0,4},{4,8},{8,12},{12,16},{16,20},{20,24},{24,28},{1,5},{5,9},{9,... | collective-permute-start | bytes 393224 | tf_op jit(solution)/shard_map/ppermute | solution.py:18
  4.7 1.1 reshape.239
  5.8 0.8 fusion.24
  6.6 0.8 constant_dynamic-slice_fusion
  7.4 0.3 multiply_cosine_fusion
  7.6 0.2 multiply_cosine_fusion.1
  7.8 1.1 %copy.38 = bf16[256,512]{0,1:T(8,128)(2,1)S(1)} copy(bf16[256,512]{1,0:T(8,128)(2,1)} %param.12) | data formatting | bytes 524288 | tf_op args[0]
  9.0 0.1 subtract_convert_fusion
  9.2 0.1 add_compare_fusion
  9.2 0.0 copy-done.3
  9.3 0.1 max.19
  9.3 0.2 copy.45
  9.5 0.1 copy.48
  9.6 0.1 fusion.22
  9.7 0.1 reduce_window_sum.11
  9.8 0.2 select_reduce_fusion
  10.0 0.6 fusion.21.sel
  10.6 0.1 broadcast_and_fusion
  10.8 0.6 pad.4.extra
  11.4 0.7 fusion.23.sel_back
  12.1 0.0 collective-permute-done
  12.1 0.1 subtract_convert_fusion.1
  12.2 0.1 copy_bitcast_fusion
  12.3 0.0 copy-start.2
  12.3 0.5 fusion.31
  12.8 0.0 copy-start.1
  12.8 0.1 broadcast_maximum_fusion
  12.9 1.3 %copy-done.1 = f32[2,4,2,128,256]{3,4,2,1,0:T(8,128)} copy-done((f32[2,4,2,128,256]{3,4,2,1,0:T(8,128)}, f32[2,4,2,128,256]{3,4,2,1,0:T(8,128)S(1)}, u32[]{:S(2)}) %copy-start.1) | copy-done | bytes 2097176
  14.2 0.3 fusion
  14.5 0.1 add_bitcast_fusion
  14.6 0.1 copy.41
  14.7 0.0 copy-done.2
  14.7 0.2 reshape.238
  14.9 0.2 copy.44
  15.1 2.1 %fusion.3 = bf16[2,128,4,2,64]{1,4,3,2,0:T(8,128)(2,1)S(1)} fusion(f32[2,4,2,128,256]{3,4,2,1,0:T(8,128)} %copy-done.1, f32[2,4,2,128]{3,2,1,0:T(2,128)S(1)} %broadcast_maximum_fusion, bf16[2,128,4,64]{1,3,2,0:T(8,128)(2,1)S(1)} %copy.45, bf16[2,128,4,64]{1,3,2,0:T(8,128)(2,1)S(1)} %copy.44, f32[2,128,4,2]{1,3,2,0:T(2,128)S(1)} %add_bitcast_fusion), kind=kOutput, calls=%fused_computation.7 | convolution fusion | flops 68943872 | bytes 2637824 | tf_op jit(solution)/shard_map/bkgqs,bskd->bkgqd/dot_general | solution.py:53
  17.1 0.3 copy.47
  17.4 0.0 copy-done
  17.4 1.7 %convolution_convert_fusion = bf16[256,2048]{1,0:T(8,128)(2,1)} fusion(bf16[512,2048]{1,0:T(8,128)(2,1)S(1)} %copy-done, bf16[64,8,2,128]{3,2,1,0:T(2,128)(2,1)S(1)} %bitcast.75), kind=kOutput, calls=%fused_computation | convolution fusion | flops 537395200 | bytes 3407872 | tf_op jit(solution)/shard_map/dot_general | solution.py:450
  19.1 87.5 %shard_map.118 = bf16[64,2048]{1,0:T(8,128)(2,1)} custom-call(bf16[4,64,2048]{2,1,0:T(8,128)(2,1)} %bitcast.73, bf16[64,2048]{1,0:T(8,128)(2,1)} %resid.1, f32[1,2048]{1,0:T(1,128)} %bitcast.79, bf16[64,128]{1,0:T(8,128)(2,1)} %pad.4.extra, bf16[128,64]{1,0:T(8,128)(2,1)} %fusion.21.sel, bf16[64,128]{1,0:T(8,128)(2,1)} %fusion.23.sel_back, ...), custom_call_target="tpu_custom_call" | custom-call | tf_op jit(solution)/shard_map/pallas_call | solution.py:363
  106.6 1.7 %copy.67 = bf16[64,2048]{1,0:T(8,128)(2,1)} copy(bf16[64,2048]{1,0:T(8,128)(2,1)} %shard_map.118) | data formatting | bytes 524288
  (21 shorter events, 0.4 us)
Async XLA Ops:
  0.0 17.4 %copy-start = (bf16[512,2048]{1,0:T(8,128)(2,1)S(1)}, bf16[512,2048]{1,0:T(8,128)(2,1)}, u32[]{:S(2)}) copy-start(bf16[512,2048]{1,0:T(8,128)(2,1)} %param.17) | copy-start | bytes 6291460
  2.1 7.1 %copy-start.3 = (f32[8]{0:T(128)S(1)}, f32[8]{0:T(128)}, u32[]{:S(2)}) copy-start(f32[8]{0:T(128)} %param.15) | copy-start | bytes 100
  2.2 9.9 %collective-permute-start = (bf16[2,128,256]{1,2,0:T(8,128)(2,1)S(1)}, bf16[2,128,256]{1,2,0:T(8,128)(2,1)S(1)}, u32[]{:S(2)}, u32[]{:S(2)}) collective-permute-start(bf16[2,128,256]{1,2,0:T(8,128)(2,1)S(1)} %pad_maximum_fusion.2), channel_id=1, source_target_pairs={{0,4},{4,8},{8,12},{12,16},{16,20},{20,24},{24,28},{1,5},{5,9},{9,... | collective-permute-start | bytes 393224 | tf_op jit(solution)/shard_map/ppermute | solution.py:18
  12.3 2.4 %copy-start.2 = (bf16[256,256]{1,0:T(8,128)(2,1)S(1)}, bf16[256,256]{1,0:T(8,128)(2,1)}, u32[]{:S(2)}) copy-start(bf16[256,256]{1,0:T(8,128)(2,1)} %param.14) | copy-start | bytes 393220
  12.8 1.4 %copy-start.1 = (f32[2,4,2,128,256]{3,4,2,1,0:T(8,128)}, f32[2,4,2,128,256]{3,4,2,1,0:T(8,128)S(1)}, u32[]{:S(2)}) copy-start(f32[2,4,2,128,256]{3,4,2,1,0:T(8,128)S(1)} %get-tuple-element.20) | copy-start | bytes 6291460
where the time goes:
time: 109 us; the launch traced here: 108 us
  Pallas kernels  87.5 us (80%)
  local copies, waits for them, and re-layouts  9.82 us (9%)
  matrix products  4.3 us (4%)
  other arithmetic  3.97 us (4%)
  starting transfers between devices  2.4 us (2%)
    pallas_call x1, Pallas kernels, group_experts(): pl.pallas_call(group_kernel, out_shape=jax.ShapeDtypeStruct((row_n, width...  87.5 us
    unnamed x12, local copies, waits for them, and re-layouts  5.3 us
    ppermute x1, starting transfers between devices, from_behind(): return lax.ppermute(block, axis, route)  2.4 us
  transfers between devices with their start and end apart: 1, of which 0 were waited for; matrix products, arithmetic and copies ran while one was open for 7% of the time, Pallas kernels for 0%

commit v1 on v0

--- a/solution.py
+++ b/solution.py
@@ -89,8 +89,13 @@
 
 
 GROUPS = 4
-TILE = 256
+TILE = 512
 MESH = pl.DeviceIdType.MESH
+VIA, ON, DIAG = 0, 1, 2
+
+
+def pieces(i):
+    return 2 if i == GROUPS - 1 else 1
 
 
 def group_kernel(
@@ -108,15 +113,17 @@
     core = lax.rem(sp, 2)
     z = sp // 2
     tp_n, row_n, width = proj.shape
-    ext_width = normed.shape[1]
     cap = outb.shape[1]
     half = GROUPS * cap
     flip1 = t + 1 - 2 * lax.rem(t, 2)
     flip2 = lax.rem(t + 2, 4)
     flip3 = lax.rem(flip1 + 2, 4)
     peer = [t, flip1, flip2, flip3]
+    via_t = flip1 + core * (flip2 - flip1)
+    on_t = flip2 + core * (flip1 - flip2)
+    near = [via_t, on_t, flip3]
     partner = sp + 1 - 2 * core
-    zoff = lambda k: lax.rem(z + k + GROUPS, GROUPS)
+    plane = [z, z + 1 - 2 * lax.rem(z, 2), lax.rem(z + 2, GROUPS), GROUPS - 1 - z]
 
     loads = [
         pltpu.make_async_copy(a, b, w_sem.at[i])
@@ -127,17 +134,20 @@
 
     barrier = pltpu.get_barrier_semaphore()
     friends = [(sp, peer[d]) for d in (1, 2, 3)]
-    friends += [(zoff(k) * 2 + core, t) for k in (1, 2, 3)] + [(partner, t)]
+    friends += [(plane[i] * 2 + core, t) for i in (1, 2, 3)] + [(partner, t)]
     for dev in friends:
         pl.semaphore_signal(barrier, inc=1, device_id=dev, device_id_type=MESH)
     pl.semaphore_wait(barrier, len(friends))
 
     sent = []
 
-    def send(src, dst, ss, rs, dev):
-        c = pltpu.make_async_remote_copy(
+    def describe(src, dst, ss, rs, dev):
+        return pltpu.make_async_remote_copy(
             src_ref=src, dst_ref=dst, send_sem=ss, recv_sem=rs, device_id=dev, device_id_type=MESH
         )
+
+    def send(src, dst, ss, rs, dev):
+        c = describe(src, dst, ss, rs, dev)
         c.start()
         sent.append(c)
         return c
@@ -168,117 +178,122 @@
         s = sel[pl.ds(pl.multiple_of(g * cap, cap), cap), :]
         return jnp.dot(s, normed[...], preferred_element_type=jnp.float32).astype(jnp.bfloat16)
 
-    order = (0, 1, 3, 2)
     ag = {}
     pt = {}
-
-    def push(d, k, tt, to):
-        ref = block(tt, core, zoff(-k))
-        ag[(d, k)] = send(ref, ref, ag_s.at[d - 1, k], ag_r.at[d - 1, k], (sp, peer[to]))
-
-    def across(d, k):
-        ref = block(peer[d], core, zoff(-k))
-        pt[(d, k)] = send(ref, ref, pt_s.at[d, k], pt_r.at[d, k], (partner, t))
-
-    disp = [None] * GROUPS
+    swap = {}
+    r2 = {}
+    disp = {}
+    bk = []
+
+    def push(d, i, tt, to):
+        ref = block(tt, core, plane[i])
+        ag[(d, i)] = send(ref, ref, ag_s.at[d, i], ag_r.at[d, i], (sp, to))
+
+    def across(d, i, tt):
+        ref = block(tt, core, plane[i])
+        pt[(d, i)] = send(ref, ref, pt_s.at[d, i], pt_r.at[d, i], (partner, t))
+
+    def dispatch(i):
+        g = plane[i]
+        outb[i] = pack(g)
+        disp[i] = send(outb.at[i], block(t, core, z), di_s.at[i], di_r.at[i], (2 * g + core, t))
 
     def spread(i):
-        k = order[i]
-        if k:
-            disp[k].wait_recv()
-        push(1, k, t, 1)
-        push(2, k, t, 2)
-        across(0, k)
+        if i:
+            disp[i].wait_recv()
+        push(VIA, i, t, via_t)
+        push(ON, i, t, on_t)
+        across(3, i, t)
 
     def relay(i):
-        k = order[i]
-        via = 1 + i % 2
-        ag[(via, k)].wait_recv()
-        push(3, k, peer[via], 3 - via)
-        across(via, k)
-        ag[(3 - via, k)].wait_recv()
-        across(3 - via, k)
+        ag[(VIA, i)].wait_recv()
+        push(DIAG, i, via_t, on_t)
+        across(VIA, i, via_t)
+
+    def other(i):
+        ag[(ON, i)].wait_recv()
+        across(ON, i, on_t)
 
     def corner(i):
-        k = order[i]
-        ag[(3, k)].wait_recv()
-        across(3, k)
+        ag[(DIAG, i)].wait_recv()
+        across(DIAG, i, flip3)
 
     def widen(i):
-        k = order[i]
-        zz = zoff(-k)
-        for d in (0, 1, 2, 3):
-            pt[(d, k)].wait_recv()
+        for d in range(4):
+            pt[(d, i)].wait_recv()
 
         @pl.loop(0, wg.shape[1] // TILE)
         def _(n):
             cols = pl.ds(pl.multiple_of(n * TILE, TILE), TILE)
-            x = rows[zz, :, :width]
+            x = rows[plane[i], :, :width]
             g = jnp.dot(x, wg[:, cols], preferred_element_type=jnp.float32)
             u = jnp.dot(x, wu[:, cols], preferred_element_type=jnp.float32)
             hid[:, cols] = (g / (1.0 + jnp.exp(-g)) * u).astype(jnp.bfloat16)
 
-    swap = {}
-
-    def narrow(i):
-        k = order[i]
-        ext = rows[zoff(-k), :, width:].astype(jnp.float32)
+    def part_cols(i, h):
+        size = width // pieces(i)
+        return pl.ds(h * size, size)
+
+    def narrow(i, h=0):
+        ext = rows[plane[i], :, width:].astype(jnp.float32)
         lane = lax.broadcasted_iota(jnp.int32, ext.shape, 1)
         mine = (lane == core) | (lane == core + 2)
         weight = jnp.sum(jnp.where(mine, ext, 0.0), -1, keepdims=True)
-
-        @pl.loop(0, width // TILE)
+        tiles = width // TILE // pieces(i)
+
+        @pl.loop(h * tiles, (h + 1) * tiles)
         def _(n):
             cols = pl.ds(pl.multiple_of(n * TILE, TILE), TILE)
             y = jnp.dot(hid[...], wd[:, cols], preferred_element_type=jnp.float32)
-            outp[k, :, cols] = (y * weight).astype(jnp.bfloat16)
-
-        other = outp.at[k, pl.ds(pl.multiple_of((1 - core) * half, half), half)]
-        swap[k] = send(other, pr.at[k], pr_s.at[k], pr_r.at[k], (partner, t))
-
-    def own(k, d):
-        off = pl.multiple_of((core * tp_n + peer[d]) * cap, cap)
-        here = pl.ds(pl.multiple_of(peer[d] * cap, cap), cap)
-        return outp[k, pl.ds(off, cap), :].astype(jnp.float32) + pr[k, here, :].astype(jnp.float32)
-
-    r2 = {}
-
-    def ship(k, d, to):
-        r2[(d, k)] = send(
-            comb.at[k, d - 1], rs2.at[k, d - 1],
-            r2_s.at[d - 1, k], r2_r.at[d - 1, k], (sp, peer[to]),
+            outp[i, :, cols] = (y * weight).astype(jnp.bfloat16)
+
+        here = part_cols(i, h)
+        other_half = outp.at[i, pl.ds(pl.multiple_of((1 - core) * half, half), half), here]
+        swap[(i, h)] = send(
+            other_half, pr.at[i, :, here], pr_s.at[i, h], pr_r.at[i, h], (partner, t)
         )
 
-    def combine(i):
-        k = order[i]
-        via = 1 + i % 2
-        swap[k].wait_recv()
-        comb[k, 2] = own(k, 3).astype(jnp.bfloat16)
-        ship(k, 3, via)
-        comb[k, via - 1] = own(k, via).astype(jnp.bfloat16)
-        ship(k, via, via)
-
-    def combine_on(i):
-        k = order[i]
-        on = 2 - i % 2
-        r2[(3, k)].wait_recv()
-        comb[k, on - 1] = (own(k, on) + rs2[k, 2].astype(jnp.float32)).astype(jnp.bfloat16)
-        ship(k, on, on)
-
-    bk = []
-
-    def finish(i):
-        k = order[i]
-        acc = own(k, 0)
-        for d in (1, 2):
-            r2[(d, k)].wait_recv()
-            acc = acc + rs2[k, d - 1].astype(jnp.float32)
-        if k:
-            ret[k] = acc.astype(jnp.bfloat16)
+    def own(i, h, tt):
+        here = part_cols(i, h)
+        mine = pl.ds(pl.multiple_of((core * tp_n + tt) * cap, cap), cap)
+        theirs = pl.ds(pl.multiple_of(tt * cap, cap), cap)
+        return outp[i, mine, here].astype(jnp.float32) + pr[i, theirs, here].astype(jnp.float32)
+
+    def ship(d, i, h, to):
+        here = part_cols(i, h)
+        r2[(d, i, h)] = send(
+            comb.at[i, d, :, here], rs2.at[i, d, :, here],
+            r2_s.at[d, i, h], r2_r.at[d, i, h], (sp, to),
+        )
+
+    def combine(i, h=0):
+        here = part_cols(i, h)
+        swap[(i, h)].wait_recv()
+        comb[i, DIAG, :, here] = own(i, h, flip3).astype(jnp.bfloat16)
+        ship(DIAG, i, h, via_t)
+        comb[i, VIA, :, here] = own(i, h, via_t).astype(jnp.bfloat16)
+        ship(VIA, i, h, via_t)
+
+    def combine_on(i, h=0):
+        here = part_cols(i, h)
+        r2[(DIAG, i, h)].wait_recv()
+        comb[i, ON, :, here] = (
+            own(i, h, on_t) + rs2[i, DIAG, :, here].astype(jnp.float32)
+        ).astype(jnp.bfloat16)
+        ship(ON, i, h, on_t)
+
+    def finish(i, h=0):
+        here = part_cols(i, h)
+        acc = own(i, h, t)
+        for d in (VIA, ON):
+            r2[(d, i, h)].wait_recv()
+            acc = acc + rs2[i, d, :, here].astype(jnp.float32)
+        if i:
+            ret[i, :, here] = acc.astype(jnp.bfloat16)
             bk.append(
                 send(
-                    ret.at[k], back.at[z], bk_s.at[k - 1], bk_r.at[k - 1],
-                    (2 * zoff(-k) + core, t),
+                    ret.at[i, :, here], back.at[z, :, here], bk_s.at[i, h], bk_r.at[i, h],
+                    (2 * plane[i] + core, t),
                 )
             )
         else:
@@ -286,45 +301,50 @@
 
     block(t, core, z)[...] = pack(z)
     spread(0)
-    for k in (1, 3, 2):
-        g = zoff(k)
-        outb[k] = pack(g)
-        disp[k] = send(
-            outb.at[k], block(t, core, z), di_s.at[k - 1], di_r.at[k - 1], (2 * g + core, t)
-        )
+    dispatch(1)
+    dispatch(2)
+    dispatch(3)
     relay(0)
+    spread(1)
+    other(0)
+    relay(1)
     corner(0)
-    spread(1)
+    spread(2)
     for c in loads:
         c.wait()
     widen(0)
-    relay(1)
-    spread(2)
+    other(1)
     narrow(0)
+    relay(2)
+    spread(3)
     corner(1)
     widen(1)
-    relay(2)
-    spread(3)
-    combine(0)
+    other(2)
     narrow(1)
+    relay(3)
     corner(2)
+    combine(1)
     widen(2)
-    relay(3)
-    combine_on(0)
-    combine(1)
+    combine_on(1)
+    other(3)
     narrow(2)
     corner(3)
-    combine_on(1)
+    combine(2)
+    finish(1)
     widen(3)
+    combine_on(2)
+    narrow(3, 0)
+    finish(2)
+    combine(3, 0)
+    narrow(3, 1)
+    combine_on(3, 0)
+    combine(3, 1)
+    combine(0)
+    finish(3, 0)
+    combine_on(3, 1)
+    combine_on(0)
+    finish(3, 1)
     finish(0)
-    combine(2)
-    narrow(3)
-    finish(1)
-    combine_on(2)
-    combine(3)
-    finish(2)
-    combine_on(3)
-    finish(3)
     for c in bk:
         c.wait_recv()
     routed = jnp.dot(
@@ -377,25 +397,25 @@
             pltpu.VMEM((row_n, ext_width), bf),
             pltpu.VMEM((GROUPS, cap, ext_width), bf),
             pltpu.VMEM((GROUPS, 2 * half, ext_width), bf),
-            dma((3,)),
-            dma((3,)),
+            dma((GROUPS,)),
+            dma((GROUPS,)),
             dma((3, GROUPS)),
             dma((3, GROUPS)),
             dma((4, GROUPS)),
             dma((4, GROUPS)),
             pltpu.VMEM((2 * half, ff), bf),
-            pltpu.VMEM((4, 2 * half, width), bf),
-            pltpu.VMEM((4, half, width), bf),
-            dma((4,)),
-            dma((4,)),
+            pltpu.VMEM((GROUPS, 2 * half, width), bf),
+            pltpu.VMEM((GROUPS, half, width), bf),
+            dma((GROUPS, 2)),
+            dma((GROUPS, 2)),
             pltpu.VMEM((GROUPS, 3, cap, width), bf),
             pltpu.VMEM((GROUPS, 3, cap, width), bf),
-            dma((3, GROUPS)),
-            dma((3, GROUPS)),
+            dma((3, GROUPS, 2)),
+            dma((3, GROUPS, 2)),
             pltpu.VMEM((GROUPS, cap, width), bf),
             pltpu.VMEM((GROUPS, cap, width), bf),
-            dma((3,)),
-            dma((3,)),
+            dma((GROUPS, 2)),
+            dma((GROUPS, 2)),
         ],
         compiler_params=pltpu.CompilerParams(
             collective_id=0, has_side_effects=True, vmem_limit_bytes=56 * 2**20

time: 109 us -> 100 us (0.917)
  Pallas kernels: 87.5 us -> 78.9 us
    pallas_call x1, Pallas kernels: 87.5 us -> 78.9 us  [group_experts(): pl.pallas_call(group_kernel, out_shape=jax.ShapeDtypeStruct((row_n, width...]
where the time goes in v1:
time: 100 us; the launch traced here: 99.7 us
  Pallas kernels  78.9 us (79%)
  local copies, waits for them, and re-layouts  9.82 us (10%)
  matrix products  4.3 us (4%)
  other arithmetic  3.97 us (4%)
  starting transfers between devices  2.4 us (2%)
    pallas_call x1, Pallas kernels, group_experts(): pl.pallas_call(group_kernel, out_shape=jax.ShapeDtypeStruct((row_n, width...  78.9 us
    unnamed x12, local copies, waits for them, and re-layouts  5.3 us
    ppermute x1, starting transfers between devices, from_behind(): return lax.ppermute(block, axis, route)  2.4 us
    dot_general x1, matrix products, attend(): jnp.einsum('bkgqs,bskd->bkgqd', exp_scores.astype(jnp.bfloat16), value_pa...  2.05 us
  transfers between devices with their start and end apart: 1, of which 0 were waited for; matrix products, arithmetic and copies ran while one was open for 7% of the time, Pallas kernels for 0%

profile of v1, /device:TPU:0, one launch (start us, length us, event | category | flops | bytes accessed | tf_op | source)
XLA Modules:
  0.0 99.7 jit_solution(10369604669739334082)
XLA Ops:
  0.0 0.0 copy-start
  0.0 1.1 %copy.33 = bf16[256,256]{0,1:T(8,128)(2,1)S(1)} copy(bf16[256,256]{1,0:T(8,128)(2,1)} %param.13) | data formatting | bytes 262144 | tf_op args[1]
  1.2 0.8 slice.50
  2.0 0.1 copy.56
  2.1 0.0 copy-start.3
  2.2 2.4 %collective-permute-start = (bf16[2,128,256]{1,2,0:T(8,128)(2,1)S(1)}, bf16[2,128,256]{1,2,0:T(8,128)(2,1)S(1)}, u32[]{:S(2)}, u32[]{:S(2)}) collective-permute-start(bf16[2,128,256]{1,2,0:T(8,128)(2,1)S(1)} %pad_maximum_fusion.2), channel_id=1, source_target_pairs={{0,4},{4,8},{8,12},{12,16},{16,20},{20,24},{24,28},{1,5},{5,9},{9,... | collective-permute-start | bytes 393224 | tf_op jit(solution)/shard_map/ppermute | solution.py:18
  4.7 1.1 %reshape.239 = bf16[2,128,4,64]{3,2,1,0:T(4,128)(2,1)S(1)} reshape(bf16[256,256]{1,0:T(8,128)(2,1)} %param.14) | data formatting | bytes 262144 | tf_op jit(solution)/shard_map/slice | solution.py:462
  5.8 0.8 fusion.24
  6.6 0.8 constant_dynamic-slice_fusion
  7.4 0.3 multiply_cosine_fusion
  7.6 0.2 multiply_cosine_fusion.1
  7.8 1.1 %copy.38 = bf16[256,512]{0,1:T(8,128)(2,1)S(1)} copy(bf16[256,512]{1,0:T(8,128)(2,1)} %param.12) | data formatting | bytes 524288 | tf_op args[0]
  9.0 0.1 subtract_convert_fusion
  9.2 0.1 add_compare_fusion
  9.2 0.0 copy-done.3
  9.3 0.1 max.19
  9.3 0.2 copy.45
  9.5 0.1 copy.48
  9.6 0.1 fusion.22
  9.7 0.1 reduce_window_sum.11
  9.8 0.2 select_reduce_fusion
  10.0 0.6 fusion.21.sel
  10.6 0.1 broadcast_and_fusion
  10.8 0.6 pad.4.extra
  11.4 0.7 fusion.23.sel_back
  12.1 0.0 collective-permute-done
  12.1 0.1 subtract_convert_fusion.1
  12.2 0.1 copy_bitcast_fusion
  12.3 0.0 copy-start.2
  12.3 0.5 fusion.31
  12.8 0.0 copy-start.1
  12.8 0.1 broadcast_maximum_fusion
  12.9 1.3 %copy-done.1 = f32[2,4,2,128,256]{3,4,2,1,0:T(8,128)} copy-done((f32[2,4,2,128,256]{3,4,2,1,0:T(8,128)}, f32[2,4,2,128,256]{3,4,2,1,0:T(8,128)S(1)}, u32[]{:S(2)}) %copy-start.1) | copy-done | bytes 2097176
  14.2 0.3 fusion
  14.5 0.1 add_bitcast_fusion
  14.6 0.1 copy.41
  14.7 0.0 copy-done.2
  14.7 0.2 reshape.238
  14.9 0.2 copy.44
  15.1 2.1 %fusion.3 = bf16[2,128,4,2,64]{1,4,3,2,0:T(8,128)(2,1)S(1)} fusion(f32[2,4,2,128,256]{3,4,2,1,0:T(8,128)} %copy-done.1, f32[2,4,2,128]{3,2,1,0:T(2,128)S(1)} %broadcast_maximum_fusion, bf16[2,128,4,64]{1,3,2,0:T(8,128)(2,1)S(1)} %copy.45, bf16[2,128,4,64]{1,3,2,0:T(8,128)(2,1)S(1)} %copy.44, f32[2,128,4,2]{1,3,2,0:T(2,128)S(1)} %add_bitcast_fusion), kind=kOutput, calls=%fused_computation.7 | convolution fusion | flops 68943872 | bytes 2637824 | tf_op jit(solution)/shard_map/bkgqs,bskd->bkgqd/dot_general | solution.py:53
  17.1 0.3 copy.47
  17.4 0.0 copy-done
  17.4 1.7 %convolution_convert_fusion = bf16[256,2048]{1,0:T(8,128)(2,1)} fusion(bf16[512,2048]{1,0:T(8,128)(2,1)S(1)} %copy-done, bf16[64,8,2,128]{3,2,1,0:T(2,128)(2,1)S(1)} %bitcast.75), kind=kOutput, calls=%fused_computation | convolution fusion | flops 537395200 | bytes 3407872 | tf_op jit(solution)/shard_map/dot_general | solution.py:470
  19.1 78.9 %shard_map.118 = bf16[64,2048]{1,0:T(8,128)(2,1)} custom-call(bf16[4,64,2048]{2,1,0:T(8,128)(2,1)} %bitcast.73, bf16[64,2048]{1,0:T(8,128)(2,1)} %resid.1, f32[1,2048]{1,0:T(1,128)} %bitcast.79, bf16[64,128]{1,0:T(8,128)(2,1)} %pad.4.extra, bf16[128,64]{1,0:T(8,128)(2,1)} %fusion.21.sel, bf16[64,128]{1,0:T(8,128)(2,1)} %fusion.23.sel_back, ...), custom_call_target="tpu_custom_call" | custom-call | tf_op jit(solution)/shard_map/pallas_call | solution.py:383
  98.1 1.7 %copy.67 = bf16[64,2048]{1,0:T(8,128)(2,1)} copy(bf16[64,2048]{1,0:T(8,128)(2,1)} %shard_map.118) | data formatting | bytes 524288
  (21 shorter events, 0.4 us)
Async XLA Ops:
  0.0 17.4 %copy-start = (bf16[512,2048]{1,0:T(8,128)(2,1)S(1)}, bf16[512,2048]{1,0:T(8,128)(2,1)}, u32[]{:S(2)}) copy-start(bf16[512,2048]{1,0:T(8,128)(2,1)} %param.17) | copy-start | bytes 6291460
  2.1 7.1 %copy-start.3 = (f32[8]{0:T(128)S(1)}, f32[8]{0:T(128)}, u32[]{:S(2)}) copy-start(f32[8]{0:T(128)} %param.15) | copy-start | bytes 100
  2.2 9.9 %collective-permute-start = (bf16[2,128,256]{1,2,0:T(8,128)(2,1)S(1)}, bf16[2,128,256]{1,2,0:T(8,128)(2,1)S(1)}, u32[]{:S(2)}, u32[]{:S(2)}) collective-permute-start(bf16[2,128,256]{1,2,0:T(8,128)(2,1)S(1)} %pad_maximum_fusion.2), channel_id=1, source_target_pairs={{0,4},{4,8},{8,12},{12,16},{16,20},{20,24},{24,28},{1,5},{5,9},{9,... | collective-permute-start | bytes 393224 | tf_op jit(solution)/shard_map/ppermute | solution.py:18
  12.3 2.4 %copy-start.2 = (bf16[256,256]{1,0:T(8,128)(2,1)S(1)}, bf16[256,256]{1,0:T(8,128)(2,1)}, u32[]{:S(2)}) copy-start(bf16[256,256]{1,0:T(8,128)(2,1)} %param.14) | copy-start | bytes 393220
  12.8 1.4 %copy-start.1 = (f32[2,4,2,128,256]{3,4,2,1,0:T(8,128)}, f32[2,4,2,128,256]{3,4,2,1,0:T(8,128)S(1)}, u32[]{:S(2)}) copy-start(f32[2,4,2,128,256]{3,4,2,1,0:T(8,128)S(1)} %get-tuple-element.20) | copy-start | bytes 6291460

commit v2 on v1

--- a/solution.py
+++ b/solution.py
@@ -1,5 +1,6 @@
 import jax
 import jax.numpy as jnp
+import numpy as np
 from jax import lax
 from jax.experimental import pallas as pl
 from jax.experimental.pallas import tpu as pltpu
@@ -90,18 +91,21 @@
 
 GROUPS = 4
 TILE = 512
+LANES = 128
 MESH = pl.DeviceIdType.MESH
 VIA, ON, DIAG = 0, 1, 2
 
 
-def pieces(i):
-    return 2 if i == GROUPS - 1 else 1
+PIECES = 2
 
 
 def group_kernel(
-    proj, resid, gain, extra, sel, sel_back, wg_hbm, wu_hbm, wd_hbm, out,
-    wg, wu, wd, w_sem,
-    rs_in, rs_s, rs_r,
+    sink, q_in, k_in, v_in, turn_row, turn_base, resid, gain, ids, weights,
+    wo_hbm, wg_hbm, wu_hbm, wd_hbm, out,
+    wo, wg, wu, wd, w_sem,
+    rim, rim_s, rim_r, asks, keys, vals, att,
+    proj, rs_in, rs_s, rs_r,
+    sel, ext,
     mid, normed, outb, rows,
     di_s, di_r, ag_s, ag_r, pt_s, pt_r,
     hid, outp, pr, pr_s, pr_r,
@@ -110,6 +114,7 @@
 ):
     sp = lax.axis_index("sp")
     t = lax.axis_index("tp")
+    sp_n = lax.axis_size("sp")
     core = lax.rem(sp, 2)
     z = sp // 2
     tp_n, row_n, width = proj.shape
@@ -121,23 +126,22 @@
     peer = [t, flip1, flip2, flip3]
     via_t = flip1 + core * (flip2 - flip1)
     on_t = flip2 + core * (flip1 - flip2)
-    near = [via_t, on_t, flip3]
     partner = sp + 1 - 2 * core
     plane = [z, z + 1 - 2 * lax.rem(z, 2), lax.rem(z + 2, GROUPS), GROUPS - 1 - z]
 
     loads = [
         pltpu.make_async_copy(a, b, w_sem.at[i])
-        for i, (a, b) in enumerate(((wg_hbm, wg), (wu_hbm, wu), (wd_hbm, wd)))
+        for i, (a, b) in enumerate(((wo_hbm, wo), (wg_hbm, wg), (wu_hbm, wu), (wd_hbm, wd)))
     ]
     for c in loads:
         c.start()
 
     barrier = pltpu.get_barrier_semaphore()
+    rim_peer = lax.rem(sp + 2 * core - 1 + sp_n, sp_n)
     friends = [(sp, peer[d]) for d in (1, 2, 3)]
-    friends += [(plane[i] * 2 + core, t) for i in (1, 2, 3)] + [(partner, t)]
+    friends += [(plane[i] * 2 + core, t) for i in (1, 2, 3)] + [(partner, t), (rim_peer, t)]
     for dev in friends:
         pl.semaphore_signal(barrier, inc=1, device_id=dev, device_id_type=MESH)
-    pl.semaphore_wait(barrier, len(friends))
 
     sent = []
 
@@ -152,31 +156,235 @@
         sent.append(c)
         return c
 
-    firsts = [
-        send(proj.at[peer[d]], rs_in.at[d - 1], rs_s.at[d - 1], rs_r.at[d - 1], (sp, peer[d]))
-        for d in (3, 1, 2)
+    bf = jnp.bfloat16
+    f32 = jnp.float32
+    local = q_in.shape[0]
+    tiles = k_in.shape[1] // LANES
+    pairs = q_in.shape[1] // LANES
+    edge = WINDOW
+    pad = keys.shape[1] - local - edge
+    span = pad + edge + row_n
+
+    at_sp = lax.broadcasted_iota(jnp.int32, turn_base.shape, 0) == sp
+    start = jnp.sum(jnp.where(at_sp, turn_base[...], 0.0), 0, keepdims=True)
+    cb, sb = start[:, :LANES], start[:, LANES:]
+    cr = turn_row[:, :LANES]
+    sr = turn_row[:, LANES:]
+    cosine = cb * cr - sb * sr
+    sine = sb * cr + cb * sr
+    spot = lax.broadcasted_iota(jnp.int32, (LANES, LANES), 0)
+    lane_i = lax.broadcasted_iota(jnp.int32, (LANES, LANES), 1)
+    swapped = jnp.where(lax.rem(lane_i, HEAD) < HEAD // 2, lane_i + HEAD // 2, lane_i - HEAD // 2)
+    exchange = (spot == swapped).astype(bf)
+
+    def turned(x, lo):
+        n = x.shape[0]
+        y = jnp.dot(x, exchange, preferred_element_type=f32)
+        return x.astype(f32) * cosine[lo : lo + n] + y * sine[lo : lo + n]
+
+    def doubled(x, ref, j, lo):
+        n = x.shape[0]
+        moved = pltpu.roll(x, HEAD, 1)
+        first = lax.broadcasted_iota(jnp.int32, x.shape, 1) < HEAD
+        ref[2 * j, lo : lo + n, :] = jnp.where(first, x, moved).astype(bf)
+        ref[2 * j + 1, lo : lo + n, :] = jnp.where(first, moved, x).astype(bf)
+
+    rim_next = lax.rem(sp + 1, sp_n)
+    rims = [
+        describe(
+            src.at[pl.ds(local - edge, edge)], rim.at[i], rim_s.at[i], rim_r.at[i], (rim_next, t)
+        )
+        for i, src in enumerate((k_in, v_in))
     ]
-    for c in firsts:
-        c.wait_recv()
-    total = resid[...].astype(jnp.float32) + (
-        proj[t].astype(jnp.float32)
-        + rs_in[0].astype(jnp.float32)
-        + rs_in[1].astype(jnp.float32)
-        + rs_in[2].astype(jnp.float32)
-    )
-    middle = total.astype(jnp.bfloat16)
+
+    def rim_out():
+        @pl.when(sp < sp_n - 1)
+        def _():
+            for c in rims:
+                c.start()
+
+    def fill(k_src, v_src, lo):
+        for j in range(tiles):
+            cols = slice(j * LANES, (j + 1) * LANES)
+            doubled(turned(k_src[:, cols], lo), keys, j, lo + pad)
+            doubled(v_src[:, cols].astype(f32), vals, j, lo + pad)
+
+    def ask():
+        lane = lax.broadcasted_iota(jnp.int32, (local, LANES), 1)
+        for j in range(pairs):
+            q = turned(q_in[:, j * LANES : (j + 1) * LANES], edge) * HEAD ** (-0.5)
+            head = [jnp.where(lane < HEAD, q, 0.0), jnp.where(lane < HEAD, 0.0, q)]
+            for i in (0, 1):
+                for b in range(tp_n):
+                    asks[b, j, i * row_n : (i + 1) * row_n, :] = head[i][
+                        b * row_n : (b + 1) * row_n
+                    ].astype(bf)
+        keys[:, :pad, :] = jnp.zeros((keys.shape[0], pad, LANES), bf)
+        vals[:, :pad, :] = jnp.zeros((keys.shape[0], pad, LANES), bf)
+
+    def fill_own():
+        fill(k_in, v_in, edge)
+
+    upper = t >= tp_n // 2
+    turn_order = [
+        jnp.where(upper, t, flip3),
+        jnp.where(upper, flip3, flip2),
+        jnp.where(upper, via_t, flip1),
+        jnp.where(upper, on_t, t),
+    ]
+
+    def attend_block(i):
+        b = turn_order[i]
+        start_at = pl.multiple_of(b * row_n, row_n)
+        shape = (2 * row_n, span)
+        row = lax.rem(lax.broadcasted_iota(jnp.int32, shape, 0), row_n)
+        col = lax.broadcasted_iota(jnp.int32, shape, 1)
+        ahead = col - row
+        key_pos = sp * local + b * row_n - pad - edge + col
+        allowed = (ahead > pad + edge - WINDOW) & (ahead <= pad + edge) & (key_pos >= 0)
+        lane = lax.broadcasted_iota(jnp.int32, (row_n, LANES), 1)
+        top = lax.broadcasted_iota(jnp.int32, (2 * row_n, 1), 0) < row_n
+        window = pl.ds(start_at, span)
+        all_j = range(pairs)
+        scores = [
+            lax.dot_general(
+                asks[b, j], keys[j, window, :], (((1,), (1,)), ((), ())),
+                preferred_element_type=f32,
+            )
+            for j in all_j
+        ]
+        scores = [jnp.where(allowed, s, -jnp.inf) for s in scores]
+        rest = [jnp.where(top, sink[2 * j], sink[2 * j + 1]) for j in all_j]
+        highest = [
+            jnp.maximum(jnp.max(scores[j], -1, keepdims=True), rest[j]) for j in all_j
+        ]
+        probs = [jnp.exp(scores[j] - highest[j]) for j in all_j]
+        mixed = [
+            jnp.dot(probs[j].astype(bf), vals[j, window, :], preferred_element_type=f32)
+            for j in all_j
+        ]
+        share = [
+            1.0 / (jnp.sum(probs[j], -1, keepdims=True) + jnp.exp(rest[j] - highest[j]))
+            for j in all_j
+        ]
+        for j in all_j:
+            m = mixed[j] * share[j]
+            att[:, j * LANES : (j + 1) * LANES] = jnp.where(
+                lane < HEAD, m[:row_n], m[row_n:]
+            ).astype(bf)
+        if i == 0:
+            loads[0].wait()
+        proj[b] = jnp.dot(att[...], wo[...], preferred_element_type=f32).astype(bf)
+
+    def give(i):
+        b = turn_order[i]
+        slot = jnp.where(b == flip3, DIAG, VIA)
+
+        @pl.when((b != t) & (b != on_t))
+        def _():
+            describe(
+                proj.at[b], rs_in.at[slot], rs_s.at[slot], rs_r.at[slot], (sp, via_t)
+            ).start()
+
+    def given(slot, to):
+        return describe(proj.at[0], rs_in.at[slot], rs_s.at[slot], rs_r.at[slot], (sp, to))
+
+    def give_on():
+        given(DIAG, via_t).wait_recv()
+        proj[on_t] = (proj[on_t].astype(f32) + rs_in[DIAG].astype(f32)).astype(bf)
+        send(proj.at[on_t], rs_in.at[ON], rs_s.at[ON], rs_r.at[ON], (sp, on_t))
+
+    def rim_in(now):
+        @pl.when(now & (sp > 0))
+        def _():
+            for c in rims:
+                c.wait_recv()
+
+        @pl.when(now & (sp == 0))
+        def _():
+            rim[...] = jnp.zeros(rim.shape, bf)
+
+        @pl.when(now)
+        def _():
+            fill(rim.at[0], rim.at[1], 0)
+
+    def slots():
+        def mine(x):
+            x = jnp.broadcast_to(x, (8, x.shape[1]))
+            x = jnp.where(t >= 2, x[:, LANES:], x[:, :LANES])
+            return jnp.where(lax.rem(t, 2) == 1, pltpu.roll(x, row_n, 1), x)
+
+        picks = [mine(ids[k : k + 1, :]) for k in (0, 1)]
+        parts = [mine(weights[k : k + 1, :]) for k in (0, 1)]
+        lane = lax.broadcasted_iota(jnp.int32, (8, LANES), 1)
+        sub = lax.broadcasted_iota(jnp.int32, (8, LANES), 0)
+        group = jnp.where(lane < row_n, picks[0] // 2, -1)
+        hit = sub == group
+        before = (spot < lane_i).astype(bf)
+        rank = jnp.dot(hit.astype(f32).astype(bf), before, preferred_element_type=f32)
+        rank = jnp.sum(jnp.where(hit, rank, 0.0), 0, keepdims=True).astype(jnp.int32)
+        slot = group[0:1] * cap + rank
+        slot = jnp.where(lane[0:1] < row_n, slot, -1)
+        chosen = (spot == jnp.broadcast_to(slot, (LANES, LANES))).astype(f32).astype(bf)
+        sel[0] = chosen
+        sel[1] = lax.dot_general(
+            (spot == lane_i).astype(f32).astype(bf), chosen, (((1,), (1,)), ((), ())),
+            preferred_element_type=f32,
+        ).astype(bf)
+        table = jnp.zeros((8, LANES), f32)
+        for p in (0, 1):
+            w = sum(jnp.where(lax.rem(picks[k], 2) == p, parts[k], 0.0) for k in (0, 1))
+            w = jnp.where(lane < row_n, w, 0.0)
+            high = w.astype(bf).astype(f32)
+            table = jnp.where(sub == p, high, table)
+            table = jnp.where(sub == p + 2, w - high, table)
+        table = jnp.concatenate([table, jnp.zeros((LANES - 8, LANES), f32)], 0).astype(bf)
+        ext[...] = lax.dot_general(
+            chosen, table, (((1,), (1,)), ((), ())), preferred_element_type=f32
+        ).astype(bf)
+
+    def meet():
+        pl.semaphore_wait(barrier, len(friends))
+
+    def gathered():
+        given(VIA, via_t).wait_recv()
+        given(ON, on_t).wait_recv()
+
+    ask()
+    slots()
+    meet()
+    rim_out()
+    fill_own()
+    attend_block(0)
+    give(0)
+    rim_in(upper)
+    attend_block(1)
+    give(1)
+    rim_in(t < tp_n // 2)
+    attend_block(2)
+    give(2)
+    attend_block(3)
+    give(3)
+    give_on()
+    gathered()
+    total = resid[...].astype(f32) + (
+        proj[t].astype(f32) + rs_in[VIA].astype(f32) + rs_in[ON].astype(f32)
+    )
+    middle = total.astype(bf)
     mid[...] = middle
-    mf = middle.astype(jnp.float32)
+    mf = middle.astype(f32)
     scale = lax.rsqrt(jnp.mean(mf * mf, -1, keepdims=True) + norm_epsilon)
-    normed[:, :width] = (mf * scale * gain[...]).astype(jnp.bfloat16)
-    normed[:, width:] = extra[...]
+    normed[...] = (mf * scale * gain[...]).astype(bf)
 
     def block(tt, cc, zz):
         return rows.at[zz, pl.ds(pl.multiple_of((cc * tp_n + tt) * cap, cap), cap)]
 
-    def pack(g):
-        s = sel[pl.ds(pl.multiple_of(g * cap, cap), cap), :]
-        return jnp.dot(s, normed[...], preferred_element_type=jnp.float32).astype(jnp.bfloat16)
+    def pack(g, ref):
+        spots = pl.ds(pl.multiple_of(g * cap, cap), cap)
+        ref[:, :width] = jnp.dot(
+            sel[0, spots, :row_n], normed[...], preferred_element_type=f32
+        ).astype(bf)
+        ref[:, width:] = ext[spots, :]
 
     ag = {}
     pt = {}
@@ -195,7 +403,7 @@
 
     def dispatch(i):
         g = plane[i]
-        outb[i] = pack(g)
+        pack(g, outb.at[i])
         disp[i] = send(outb.at[i], block(t, core, z), di_s.at[i], di_r.at[i], (2 * g + core, t))
 
     def spread(i):
@@ -218,33 +426,35 @@
         ag[(DIAG, i)].wait_recv()
         across(DIAG, i, flip3)
 
-    def widen(i):
-        for d in range(4):
-            pt[(d, i)].wait_recv()
-
-        @pl.loop(0, wg.shape[1] // TILE)
-        def _(n):
-            cols = pl.ds(pl.multiple_of(n * TILE, TILE), TILE)
-            x = rows[plane[i], :, :width]
-            g = jnp.dot(x, wg[:, cols], preferred_element_type=jnp.float32)
-            u = jnp.dot(x, wu[:, cols], preferred_element_type=jnp.float32)
-            hid[:, cols] = (g / (1.0 + jnp.exp(-g)) * u).astype(jnp.bfloat16)
+    def widen(i, h):
+        if h == 0:
+            for d in range(4):
+                pt[(d, i)].wait_recv()
+        if i == 0 and h == 0:
+            for c in loads[1:]:
+                c.wait()
+        size = wg.shape[1] // PIECES
+        cols = pl.ds(h * size, size)
+        x = rows[plane[i], :, :width]
+        g = jnp.dot(x, wg[:, cols], preferred_element_type=jnp.float32)
+        u = jnp.dot(x, wu[:, cols], preferred_element_type=jnp.float32)
+        hid[i, :, cols] = (g / (1.0 + jnp.exp(-g)) * u).astype(jnp.bfloat16)
 
     def part_cols(i, h):
-        size = width // pieces(i)
+        size = width // PIECES
         return pl.ds(h * size, size)
 
-    def narrow(i, h=0):
+    def narrow(i, h):
         ext = rows[plane[i], :, width:].astype(jnp.float32)
         lane = lax.broadcasted_iota(jnp.int32, ext.shape, 1)
         mine = (lane == core) | (lane == core + 2)
         weight = jnp.sum(jnp.where(mine, ext, 0.0), -1, keepdims=True)
-        tiles = width // TILE // pieces(i)
+        tiles = width // TILE // PIECES
 
         @pl.loop(h * tiles, (h + 1) * tiles)
         def _(n):
             cols = pl.ds(pl.multiple_of(n * TILE, TILE), TILE)
-            y = jnp.dot(hid[...], wd[:, cols], preferred_element_type=jnp.float32)
+            y = jnp.dot(hid[i], wd[:, cols], preferred_element_type=jnp.float32)
             outp[i, :, cols] = (y * weight).astype(jnp.bfloat16)
 
         here = part_cols(i, h)
@@ -266,7 +476,7 @@
             r2_s.at[d, i, h], r2_r.at[d, i, h], (sp, to),
         )
 
-    def combine(i, h=0):
+    def combine(i, h):
         here = part_cols(i, h)
         swap[(i, h)].wait_recv()
         comb[i, DIAG, :, here] = own(i, h, flip3).astype(jnp.bfloat16)
@@ -274,7 +484,7 @@
         comb[i, VIA, :, here] = own(i, h, via_t).astype(jnp.bfloat16)
         ship(VIA, i, h, via_t)
 
-    def combine_on(i, h=0):
+    def combine_on(i, h):
         here = part_cols(i, h)
         r2[(DIAG, i, h)].wait_recv()
         comb[i, ON, :, here] = (
@@ -282,7 +492,7 @@
         ).astype(jnp.bfloat16)
         ship(ON, i, h, on_t)
 
-    def finish(i, h=0):
+    def finish(i, h):
         here = part_cols(i, h)
         acc = own(i, h, t)
         for d in (VIA, ON):
@@ -297,104 +507,140 @@
                 )
             )
         else:
-            back[z] = acc.astype(jnp.bfloat16)
-
-    block(t, core, z)[...] = pack(z)
+            back[z, :, here] = acc.astype(jnp.bfloat16)
+
+    pack(z, block(t, core, z))
     spread(0)
     dispatch(1)
     dispatch(2)
     dispatch(3)
     relay(0)
+    other(0)
     spread(1)
-    other(0)
+    spread(2)
+    corner(0)
     relay(1)
-    corner(0)
-    spread(2)
-    for c in loads:
-        c.wait()
-    widen(0)
+    widen(0, 0)
     other(1)
-    narrow(0)
+    widen(0, 1)
     relay(2)
     spread(3)
+    narrow(0, 0)
     corner(1)
-    widen(1)
     other(2)
-    narrow(1)
+    narrow(0, 1)
+    widen(1, 0)
+    combine(0, 0)
+    widen(1, 1)
+    corner(2)
+    narrow(1, 0)
     relay(3)
-    corner(2)
-    combine(1)
-    widen(2)
-    combine_on(1)
+    widen(2, 0)
+    widen(2, 1)
+    combine(1, 0)
     other(3)
-    narrow(2)
+    narrow(2, 0)
+    combine(0, 1)
     corner(3)
-    combine(2)
-    finish(1)
-    widen(3)
-    combine_on(2)
+    narrow(2, 1)
+    combine(2, 0)
+    widen(3, 0)
+    combine_on(1, 0)
+    combine(2, 1)
+    widen(3, 1)
     narrow(3, 0)
-    finish(2)
+    combine_on(2, 0)
+    narrow(3, 1)
     combine(3, 0)
-    narrow(3, 1)
+    finish(1, 0)
+    narrow(1, 1)
+    combine(3, 1)
+    combine(1, 1)
+    finish(2, 0)
     combine_on(3, 0)
-    combine(3, 1)
-    combine(0)
+    combine_on(3, 1)
+    combine_on(2, 1)
+    combine_on(1, 1)
     finish(3, 0)
-    combine_on(3, 1)
-    combine_on(0)
     finish(3, 1)
-    finish(0)
+    combine_on(0, 0)
+    finish(2, 1)
+    finish(1, 1)
+    combine_on(0, 1)
+    finish(0, 0)
+    finish(0, 1)
     for c in bk:
         c.wait_recv()
     routed = jnp.dot(
-        sel_back[...], back[...].reshape(half, width), preferred_element_type=jnp.float32
+        sel[1, :row_n, :], back[...].reshape(half, width), preferred_element_type=f32
     )
     out[...] = (mid[...].astype(jnp.float32) + routed).astype(jnp.bfloat16)
     for c in sent:
         c.wait_send()
-
-
-def group_experts(projected, residual, norm_gain, own_ids, own_weights, gate, up, down):
+    for slot in (VIA, DIAG):
+        given(slot, via_t).wait_send()
+
+    @pl.when(sp < sp_n - 1)
+    def _():
+        for c in rims:
+            c.wait_send()
+
+
+def group_layer(
+    queries, key_rows, values, sink_logits, residual, out_weight, norm_gain, expert_ids,
+    route_weight, gate, up, down,
+):
     row_n, width = residual.shape
+    local = queries.shape[0]
     tp_n = lax.axis_size("tp")
     expert_n = lax.axis_size("sp")
     cap = 2 * max(1, 2 * row_n // expert_n)
-    group = own_ids[:, 0] // 2
-    onehot = (group[:, None] == jnp.arange(GROUPS, dtype=jnp.int32)[None, :]).astype(jnp.int32)
-    rank_of = jnp.sum(jnp.cumsum(onehot, 0) * onehot, 1) - 1
-    slot = group * cap + rank_of
-    hit = jnp.arange(GROUPS * cap, dtype=jnp.int32)[:, None] == slot[None, :]
-    sel = hit.astype(jnp.bfloat16)
-    odd = lax.rem(own_ids, 2)
-    pair = jnp.stack(
-        [jnp.sum(jnp.where(odd == p, own_weights, 0.0), 1) for p in (0, 1)], 1
-    )
-    high = pair.astype(jnp.bfloat16)
-    low = (pair - high.astype(jnp.float32)).astype(jnp.bfloat16)
-    extra = jnp.pad(jnp.concatenate([high, low], 1), ((0, 0), (0, 124)))
-    ext_width = width + 128
+    ext_width = width + LANES
     ff = gate.shape[-1]
     half = GROUPS * cap
+    kv_heads = key_rows.shape[1] // HEAD
+    frequency = 10000.0 ** (-(np.arange(LANES) % (HEAD // 2)) * 2.0 / HEAD)
+    sign = np.where(np.arange(LANES) % HEAD < HEAD // 2, -1.0, 1.0)
+
+    def turns(positions):
+        angle = positions[:, None] * frequency[None, :]
+        return jnp.asarray(
+            np.concatenate([np.cos(angle), np.sin(angle) * sign], 1), jnp.float32
+        )
+
+    turn_row = turns(np.arange(local + WINDOW) - float(WINDOW))
+    turn_base = turns(np.arange(expert_n) * float(local))
     bf = jnp.bfloat16
     dma = pltpu.SemaphoreType.DMA
     vmem = pl.BlockSpec(memory_space=pltpu.VMEM)
+    smem = pl.BlockSpec(memory_space=pltpu.SMEM)
     hbm = pl.BlockSpec(memory_space=pl.ANY)
     return pl.pallas_call(
         group_kernel,
         out_shape=jax.ShapeDtypeStruct((row_n, width), bf),
-        in_specs=[vmem] * 6 + [hbm] * 3,
+        in_specs=[smem] + [vmem] * 9 + [hbm] * 4,
         out_specs=vmem,
         scratch_shapes=[
+            pltpu.VMEM(out_weight.shape, bf),
             pltpu.VMEM((width, ff), bf),
             pltpu.VMEM((width, ff), bf),
             pltpu.VMEM((ff, width), bf),
-            dma((3,)),
+            dma((4,)),
+            pltpu.VMEM((2, WINDOW, key_rows.shape[1]), bf),
+            dma((2,)),
+            dma((2,)),
+            pltpu.VMEM((tp_n, queries.shape[1] // LANES, 2 * row_n, LANES), bf),
+            pltpu.VMEM((kv_heads, local + WINDOW + row_n, LANES), bf),
+            pltpu.VMEM((kv_heads, local + WINDOW + row_n, LANES), bf),
+            pltpu.VMEM((row_n, queries.shape[1]), bf),
+            pltpu.VMEM((tp_n, row_n, width), bf),
             pltpu.VMEM((3, row_n, width), bf),
             dma((3,)),
             dma((3,)),
+            pltpu.VMEM((2, LANES, LANES), bf),
+            pltpu.VMEM((LANES, LANES), bf),
             pltpu.VMEM((row_n, width), bf),
-            pltpu.VMEM((row_n, ext_width), bf),
+            pltpu.VMEM((row_n, width), bf),
             pltpu.VMEM((GROUPS, cap, ext_width), bf),
             pltpu.VMEM((GROUPS, 2 * half, ext_width), bf),
             dma((GROUPS,)),
@@ -403,7 +649,7 @@
             dma((3, GROUPS)),
             dma((4, GROUPS)),
             dma((4, GROUPS)),
-            pltpu.VMEM((2 * half, ff), bf),
+            pltpu.VMEM((GROUPS, 2 * half, ff), bf),
             pltpu.VMEM((GROUPS, 2 * half, width), bf),
             pltpu.VMEM((GROUPS, half, width), bf),
             dma((GROUPS, 2)),
@@ -418,11 +664,11 @@
             dma((GROUPS, 2)),
         ],
         compiler_params=pltpu.CompilerParams(
-            collective_id=0, has_side_effects=True, vmem_limit_bytes=56 * 2**20
+            collective_id=0, has_side_effects=True, vmem_limit_bytes=60 * 2**20
         ),
     )(
-        projected.reshape(tp_n, row_n, width), residual, norm_gain[None], extra, sel,
-        sel.T, gate[0], up[0], down[0],
+        sink_logits, queries, key_rows, values, turn_row, turn_base, residual, norm_gain[None],
+        expert_ids.T, route_weight.T, out_weight, gate[0], up[0], down[0],
     )
 
 
@@ -441,6 +687,11 @@
     down_proj,
 ):
     local_len = queries.shape[0]
+    if lax.axis_size("tp") == 4 and lax.axis_size("sp") == 2 * GROUPS:
+        return group_layer(
+            queries, key_rows, values, sink_logits, residual, out_weight, norm_gain,
+            expert_ids, route_weight, gate_proj, up_proj, down_proj,
+        )
     q_heads = sink_logits.shape[0]
     kv_heads = key_rows.shape[1] // HEAD
     group_size = q_heads // kv_heads
@@ -465,19 +716,6 @@
     tok_rows = residual.shape[0]
     tp_count = lax.axis_size("tp")
     tp_index = lax.axis_index("tp")
-    if tp_count == 4 and lax.axis_size("sp") == 2 * GROUPS:
-        return group_experts(
-            jnp.dot(attended, out_weight, preferred_element_type=jnp.float32).astype(
-                jnp.bfloat16
-            ),
-            residual,
-            norm_gain,
-            lax.dynamic_slice_in_dim(expert_ids, tp_index * tok_rows, tok_rows, 0),
-            lax.dynamic_slice_in_dim(route_weight, tp_index * tok_rows, tok_rows, 0),
-            gate_proj,
-            up_proj,
-            down_proj,
-        )
     projected = lax.psum_scatter(
         jnp.dot(attended, out_weight, preferred_element_type=jnp.float32).astype(jnp.bfloat16),
         "tp",

time: 100 us -> 77.9 us (0.78)
  local copies, waits for them, and re-layouts: 9.82 us -> 1.67 us
  matrix products: 4.3 us -> 0 us
  other arithmetic: 3.97 us -> 0 us
  Pallas kernels: 78.9 us -> 76.1 us
  starting transfers between devices: 2.4 us -> 0 us
    dot_general x3 -> x0, matrix products: 4.3 us -> none  [the longest x1 2.05 us: attend(): jnp.einsum('bkgqs,bskd->bkgqd', exp_scores.astype(jnp.bfloat16), value_pa...]
    unnamed x12 -> x1, local copies, waits for them, and re-layouts: 5.3 us -> 1.67 us
    pallas_call x1, Pallas kernels: 78.9 us -> 76.1 us  [group_layer(): pl.pallas_call(group_kernel, out_shape=jax.ShapeDtypeStruct((row_n, width...]
    slice x6 -> x0, local copies, waits for them, and re-layouts: 2.46 us -> none  [the longest x4 1.55 us: per_device(): value_pairs = jnp.concatenate([value_blocks[:-1], value_blocks[1:]], 1)]
    ppermute x1 -> x0, starting transfers between devices: 2.4 us -> none  [from_behind(): return lax.ppermute(block, axis, route)]
    convert_element_type x8 -> x0, other arithmetic: 1.44 us -> none  [the longest x2 1.31 us: group_experts(): sel = hit.astype(jnp.bfloat16)]
    reduce_sum x3 -> x0, other arithmetic: 1.29 us -> none  [the longest x1 0.79 us: group_experts(): jnp.sum(jnp.where(odd == p, own_weights, 0.0), 1)]
  transfers between devices with their start and end apart: 1 -> 0, of which waited for: 0 -> 0; matrix products, arithmetic and copies ran while one was open for 7% -> 0% of each run, Pallas kernels for 0% -> 0%
where the time goes in v2:
time: 77.9 us; the launch traced here: 77.8 us
  Pallas kernels  76.1 us (98%)
  local copies, waits for them, and re-layouts  1.67 us (2%)
    pallas_call x1, Pallas kernels, group_layer(): pl.pallas_call(group_kernel, out_shape=jax.ShapeDtypeStruct((row_n, width...  76.1 us
    unnamed x1, local copies, waits for them, and re-layouts  1.67 us

profile of v2, /device:TPU:0, one launch (start us, length us, event | category | flops | bytes accessed | tf_op | source)
XLA Modules:
  0.0 77.8 jit_solution(8240084924363642358)
XLA Ops:
  0.0 76.1 %shard_map.136 = bf16[64,2048]{1,0:T(8,128)(2,1)} custom-call(f32[8]{0:T(128)} %sink.1, bf16[256,512]{1,0:T(8,128)(2,1)} %q_in.1, bf16[256,256]{1,0:T(8,128)(2,1)} %k_in.1, bf16[256,256]{1,0:T(8,128)(2,1)} %v_in.1, f32[384,256]{1,0:T(8,128)} %constant.4.clone.turn_row, f32[8,256]{1,0:T(8,128)} %constant.5.clone.turn_base, bf16[64,2048]{1,0:T(8,128)(2,1)} %resid.1, ...), custom_call_target="tpu_custom_call" | custom-call | tf_op jit(solution)/shard_map/pallas_call | solution.py:618
  76.1 1.7 %copy.16 = bf16[64,2048]{1,0:T(8,128)(2,1)} copy(bf16[64,2048]{1,0:T(8,128)(2,1)} %shard_map.136) | data formatting | bytes 524288

commit v3 on v2

--- a/solution.py
+++ b/solution.py
@@ -100,8 +100,9 @@
 
 
 def group_kernel(
-    sink, q_in, k_in, v_in, turn_row, turn_base, resid, gain, ids, weights,
+    sink_hbm, q_hbm, k_hbm, v_hbm, row_hbm, base_hbm, resid_hbm, gain_hbm, ids_hbm, weights_hbm,
     wo_hbm, wg_hbm, wu_hbm, wd_hbm, out,
+    sink, q_in, k_in, v_in, turn_row, turn_base, resid, gain, ids, weights, in_sem,
     wo, wg, wu, wd, w_sem,
     rim, rim_s, rim_r, asks, keys, vals, att,
     proj, rs_in, rs_s, rs_r,
@@ -129,19 +130,25 @@
     partner = sp + 1 - 2 * core
     plane = [z, z + 1 - 2 * lax.rem(z, 2), lax.rem(z + 2, GROUPS), GROUPS - 1 - z]
 
-    loads = [
-        pltpu.make_async_copy(a, b, w_sem.at[i])
-        for i, (a, b) in enumerate(((wo_hbm, wo), (wg_hbm, wg), (wu_hbm, wu), (wd_hbm, wd)))
-    ]
-    for c in loads:
-        c.start()
-
     barrier = pltpu.get_barrier_semaphore()
     rim_peer = lax.rem(sp + 2 * core - 1 + sp_n, sp_n)
     friends = [(sp, peer[d]) for d in (1, 2, 3)]
     friends += [(plane[i] * 2 + core, t) for i in (1, 2, 3)] + [(partner, t), (rim_peer, t)]
     for dev in friends:
         pl.semaphore_signal(barrier, inc=1, device_id=dev, device_id_type=MESH)
+
+    moves = (
+        (row_hbm, turn_row), (base_hbm, turn_base), (q_hbm, q_in), (k_hbm, k_in), (v_hbm, v_in),
+        (ids_hbm, ids), (weights_hbm, weights), (sink_hbm, sink),
+        (resid_hbm, resid), (gain_hbm, gain),
+    )
+    feeds = [pltpu.make_async_copy(a, b, in_sem.at[i]) for i, (a, b) in enumerate(moves)]
+    loads = [
+        pltpu.make_async_copy(a, b, w_sem.at[i])
+        for i, (a, b) in enumerate(((wo_hbm, wo), (wg_hbm, wg), (wu_hbm, wu), (wd_hbm, wd)))
+    ]
+    for c in feeds + loads:
+        c.start()
 
     sent = []
 
@@ -165,6 +172,8 @@
     pad = keys.shape[1] - local - edge
     span = pad + edge + row_n
 
+    for c in feeds[:-2]:
+        c.wait()
     at_sp = lax.broadcasted_iota(jnp.int32, turn_base.shape, 0) == sp
     start = jnp.sum(jnp.where(at_sp, turn_base[...], 0.0), 0, keepdims=True)
     cb, sb = start[:, :LANES], start[:, LANES:]
@@ -229,8 +238,8 @@
     turn_order = [
         jnp.where(upper, t, flip3),
         jnp.where(upper, flip3, flip2),
-        jnp.where(upper, via_t, flip1),
-        jnp.where(upper, on_t, t),
+        flip1,
+        jnp.where(upper, flip2, t),
     ]
 
     def attend_block(i):
@@ -276,23 +285,36 @@
             loads[0].wait()
         proj[b] = jnp.dot(att[...], wo[...], preferred_element_type=f32).astype(bf)
 
+    lead = [via_t, on_t]
+
+    def part(h):
+        size = width // 2
+        return slice(h * size, (h + 1) * size)
+
+    def given(slot, h, b, to):
+        return describe(
+            proj.at[b, :, part(h)], rs_in.at[slot, :, part(h)],
+            rs_s.at[slot, h], rs_r.at[slot, h], (sp, to),
+        )
+
     def give(i):
         b = turn_order[i]
         slot = jnp.where(b == flip3, DIAG, VIA)
-
-        @pl.when((b != t) & (b != on_t))
-        def _():
-            describe(
-                proj.at[b], rs_in.at[slot], rs_s.at[slot], rs_r.at[slot], (sp, via_t)
-            ).start()
-
-    def given(slot, to):
-        return describe(proj.at[0], rs_in.at[slot], rs_s.at[slot], rs_r.at[slot], (sp, to))
-
-    def give_on():
-        given(DIAG, via_t).wait_recv()
-        proj[on_t] = (proj[on_t].astype(f32) + rs_in[DIAG].astype(f32)).astype(bf)
-        send(proj.at[on_t], rs_in.at[ON], rs_s.at[ON], rs_r.at[ON], (sp, on_t))
+        for h in (0, 1):
+
+            @pl.when((b == flip3) | (b == lead[h]))
+            def _():
+                given(slot, h, b, lead[h]).start()
+
+    def give_on(h):
+        given(DIAG, h, 0, lead[h]).wait_recv()
+        b = lead[1 - h]
+        proj[b, :, part(h)] = (
+            proj[b, :, part(h)].astype(f32) + rs_in[DIAG, :, part(h)].astype(f32)
+        ).astype(bf)
+        c = given(ON, h, b, b)
+        c.start()
+        sent.append(c)
 
     def rim_in(now):
         @pl.when(now & (sp > 0))
@@ -347,8 +369,9 @@
         pl.semaphore_wait(barrier, len(friends))
 
     def gathered():
-        given(VIA, via_t).wait_recv()
-        given(ON, on_t).wait_recv()
+        for h in (0, 1):
+            given(VIA, h, 0, lead[h]).wait_recv()
+            given(ON, h, 0, lead[1 - h]).wait_recv()
 
     ask()
     slots()
@@ -365,8 +388,11 @@
     give(2)
     attend_block(3)
     give(3)
-    give_on()
+    give_on(0)
+    give_on(1)
     gathered()
+    for c in feeds[-2:]:
+        c.wait()
     total = resid[...].astype(f32) + (
         proj[t].astype(f32) + rs_in[VIA].astype(f32) + rs_in[ON].astype(f32)
     )
@@ -574,11 +600,12 @@
     routed = jnp.dot(
         sel[1, :row_n, :], back[...].reshape(half, width), preferred_element_type=f32
     )
-    out[...] = (mid[...].astype(jnp.float32) + routed).astype(jnp.bfloat16)
+    out[...] = mid[...].astype(f32) + routed
     for c in sent:
         c.wait_send()
-    for slot in (VIA, DIAG):
-        given(slot, via_t).wait_send()
+    for h in (0, 1):
+        for slot in (VIA, DIAG):
+            given(slot, h, 0, lead[h]).wait_send()
 
     @pl.when(sp < sp_n - 1)
     def _():
@@ -613,14 +640,24 @@
     bf = jnp.bfloat16
     dma = pltpu.SemaphoreType.DMA
     vmem = pl.BlockSpec(memory_space=pltpu.VMEM)
-    smem = pl.BlockSpec(memory_space=pltpu.SMEM)
-    hbm = pl.BlockSpec(memory_space=pl.ANY)
-    return pl.pallas_call(
+    hbm = pl.BlockSpec(memory_space=pltpu.HBM)
+    total = pl.pallas_call(
         group_kernel,
-        out_shape=jax.ShapeDtypeStruct((row_n, width), bf),
-        in_specs=[smem] + [vmem] * 9 + [hbm] * 4,
+        out_shape=jax.ShapeDtypeStruct((row_n, width), jnp.float32),
+        in_specs=[hbm] * 14,
         out_specs=vmem,
         scratch_shapes=[
+            pltpu.SMEM(sink_logits.shape, jnp.float32),
+            pltpu.VMEM(queries.shape, bf),
+            pltpu.VMEM(key_rows.shape, bf),
+            pltpu.VMEM(values.shape, bf),
+            pltpu.VMEM(turn_row.shape, jnp.float32),
+            pltpu.VMEM(turn_base.shape, jnp.float32),
+            pltpu.VMEM(residual.shape, bf),
+            pltpu.VMEM((1, width), jnp.float32),
+            pltpu.VMEM(expert_ids.shape[::-1], jnp.int32),
+            pltpu.VMEM(route_weight.shape[::-1], jnp.float32),
+            dma((10,)),
             pltpu.VMEM(out_weight.shape, bf),
             pltpu.VMEM((width, ff), bf),
             pltpu.VMEM((width, ff), bf),
@@ -635,8 +672,8 @@
             pltpu.VMEM((row_n, queries.shape[1]), bf),
             pltpu.VMEM((tp_n, row_n, width), bf),
             pltpu.VMEM((3, row_n, width), bf),
-            dma((3,)),
-            dma((3,)),
+            dma((3, 2)),
+            dma((3, 2)),
             pltpu.VMEM((2, LANES, LANES), bf),
             pltpu.VMEM((LANES, LANES), bf),
             pltpu.VMEM((row_n, width), bf),
@@ -664,12 +701,18 @@
             dma((GROUPS, 2)),
         ],
         compiler_params=pltpu.CompilerParams(
-            collective_id=0, has_side_effects=True, vmem_limit_bytes=60 * 2**20
+            collective_id=0, has_side_effects=True, vmem_limit_bytes=50 * 2**20
         ),
     )(
-        sink_logits, queries, key_rows, values, turn_row, turn_base, residual, norm_gain[None],
-        expert_ids.T, route_weight.T, out_weight, gate[0], up[0], down[0],
-    )
+        *(
+            pltpu.with_memory_space_constraint(x, pltpu.HBM)
+            for x in (
+                sink_logits, queries, key_rows, values, turn_row, turn_base, residual,
+                norm_gain[None], expert_ids.T, route_weight.T, out_weight, gate[0], up[0], down[0],
+            )
+        )
+    )
+    return total.astype(bf)
 
 
 def per_device(

time: 77.9 us -> 70.8 us (0.909)
  Pallas kernels: 76.1 us -> 69.9 us
  local copies, waits for them, and re-layouts: 1.67 us -> 0 us
    pallas_call x1, Pallas kernels: 76.1 us -> 69.9 us  [group_layer(): pl.pallas_call(group_kernel, out_shape=jax.ShapeDtypeStruct((row_n, width...]
    unnamed x1 -> x0, local copies, waits for them, and re-layouts: 1.67 us -> none
where the time goes in v3:
time: 70.8 us; the launch traced here: 70.6 us
  Pallas kernels  69.9 us (99%)
  other arithmetic  0.73 us (1%)
    pallas_call x1, Pallas kernels, group_layer(): pl.pallas_call(group_kernel, out_shape=jax.ShapeDtypeStruct((row_n, width...  69.9 us

profile of v3, /device:TPU:0, one launch (start us, length us, event | category | flops | bytes accessed | tf_op | source)
XLA Modules:
  0.0 70.6 jit_solution(2613550203222888618)
XLA Ops:
  0.0 69.9 %shard_map.136 = f32[64,2048]{1,0:T(8,128)S(1)} custom-call(f32[8]{0:T(128)} %sink_hbm.1, bf16[256,512]{1,0:T(8,128)(2,1)} %q_hbm.1, bf16[256,256]{1,0:T(8,128)(2,1)} %k_hbm.1, bf16[256,256]{1,0:T(8,128)(2,1)} %v_hbm.1, f32[384,256]{1,0:T(8,128)} %constant.4.clone.row_hbm, f32[8,256]{1,0:T(8,128)} %constant.5.clone.base_hbm, bf16[64,2048]{1,0:T(8,128)(2,1)} %resid_hbm.1, ...), custom_call_target="tpu_custom_call" | custom-call | tf_op jit(solution)/shard_map/pallas_call | solution.py:644
  69.9 0.7 %convert_element_type.3 = bf16[64,2048]{1,0:T(8,128)(2,1)} convert(f32[64,2048]{1,0:T(8,128)S(1)} %shard_map.136) | non-fusion elementwise | flops 131072 | bytes 786432 | tf_op jit(solution)/shard_map/convert_element_type | solution.py:715

commit v4 on v3

--- a/solution.py
+++ b/solution.py
@@ -90,7 +90,6 @@
 
 
 GROUPS = 4
-TILE = 512
 LANES = 128
 MESH = pl.DeviceIdType.MESH
 VIA, ON, DIAG = 0, 1, 2
@@ -374,10 +373,9 @@
             given(ON, h, 0, lead[1 - h]).wait_recv()
 
     ask()
-    slots()
+    fill_own()
     meet()
     rim_out()
-    fill_own()
     attend_block(0)
     give(0)
     rim_in(upper)
@@ -388,6 +386,7 @@
     give(2)
     attend_block(3)
     give(3)
+    slots()
     give_on(0)
     give_on(1)
     gathered()
@@ -402,8 +401,11 @@
     scale = lax.rsqrt(jnp.mean(mf * mf, -1, keepdims=True) + norm_epsilon)
     normed[...] = (mf * scale * gain[...]).astype(bf)
 
-    def block(tt, cc, zz):
-        return rows.at[zz, pl.ds(pl.multiple_of((cc * tp_n + tt) * cap, cap), cap)]
+    def block(tt, cc, zz, g=None):
+        first = pl.multiple_of((cc * tp_n + tt) * cap, cap)
+        if g is None:
+            return rows.at[zz, pl.ds(first, cap)]
+        return rows.at[zz, pl.ds(pl.multiple_of(first + g * (cap // 2), cap // 2), cap // 2)]
 
     def pack(g, ref):
         spots = pl.ds(pl.multiple_of(g * cap, cap), cap)
@@ -417,11 +419,12 @@
     swap = {}
     r2 = {}
     disp = {}
-    bk = []
-
-    def push(d, i, tt, to):
-        ref = block(tt, core, plane[i])
-        ag[(d, i)] = send(ref, ref, ag_s.at[d, i], ag_r.at[d, i], (sp, to))
+    bk = {}
+
+    def push(step, g, half_i, i, tt, to):
+        ref = block(tt, core, plane[i], half_i)
+        n = 2 * step + g
+        ag[(step, g, i)] = send(ref, ref, ag_s.at[n, i], ag_r.at[n, i], (sp, to))
 
     def across(d, i, tt):
         ref = block(tt, core, plane[i])
@@ -435,22 +438,25 @@
     def spread(i):
         if i:
             disp[i].wait_recv()
-        push(VIA, i, t, via_t)
-        push(ON, i, t, on_t)
+        for g in (0, 1):
+            push(0, g, g, i, t, lead[g])
+        for g in (0, 1):
+            push(1, g, 1 - g, i, t, lead[g])
         across(3, i, t)
 
-    def relay(i):
-        ag[(VIA, i)].wait_recv()
-        push(DIAG, i, via_t, on_t)
-        across(VIA, i, via_t)
+    def relay(i, g):
+        ag[(0, g, i)].wait_recv()
+        push(2, g, g, i, lead[g], lead[1 - g])
 
     def other(i):
-        ag[(ON, i)].wait_recv()
-        across(ON, i, on_t)
+        for g in (0, 1):
+            ag[(1, g, i)].wait_recv()
+            across(g, i, lead[g])
 
     def corner(i):
-        ag[(DIAG, i)].wait_recv()
-        across(DIAG, i, flip3)
+        for g in (0, 1):
+            ag[(2, g, i)].wait_recv()
+        across(2, i, flip3)
 
     def widen(i, h):
         if h == 0:
@@ -475,13 +481,9 @@
         lane = lax.broadcasted_iota(jnp.int32, ext.shape, 1)
         mine = (lane == core) | (lane == core + 2)
         weight = jnp.sum(jnp.where(mine, ext, 0.0), -1, keepdims=True)
-        tiles = width // TILE // PIECES
-
-        @pl.loop(h * tiles, (h + 1) * tiles)
-        def _(n):
-            cols = pl.ds(pl.multiple_of(n * TILE, TILE), TILE)
-            y = jnp.dot(hid[i], wd[:, cols], preferred_element_type=jnp.float32)
-            outp[i, :, cols] = (y * weight).astype(jnp.bfloat16)
+        cols = part_cols(i, h)
+        y = jnp.dot(hid[i], wd[:, cols], preferred_element_type=jnp.float32)
+        outp[i, :, cols] = (y * weight).astype(jnp.bfloat16)
 
         here = part_cols(i, h)
         other_half = outp.at[i, pl.ds(pl.multiple_of((1 - core) * half, half), half), here]
@@ -506,17 +508,17 @@
         here = part_cols(i, h)
         swap[(i, h)].wait_recv()
         comb[i, DIAG, :, here] = own(i, h, flip3).astype(jnp.bfloat16)
-        ship(DIAG, i, h, via_t)
-        comb[i, VIA, :, here] = own(i, h, via_t).astype(jnp.bfloat16)
-        ship(VIA, i, h, via_t)
+        ship(DIAG, i, h, lead[h])
+        comb[i, VIA, :, here] = own(i, h, lead[h]).astype(jnp.bfloat16)
+        ship(VIA, i, h, lead[h])
 
     def combine_on(i, h):
         here = part_cols(i, h)
         r2[(DIAG, i, h)].wait_recv()
         comb[i, ON, :, here] = (
-            own(i, h, on_t) + rs2[i, DIAG, :, here].astype(jnp.float32)
+            own(i, h, lead[1 - h]) + rs2[i, DIAG, :, here].astype(jnp.float32)
         ).astype(jnp.bfloat16)
-        ship(ON, i, h, on_t)
+        ship(ON, i, h, lead[1 - h])
 
     def finish(i, h):
         here = part_cols(i, h)
@@ -526,12 +528,11 @@
             acc = acc + rs2[i, d, :, here].astype(jnp.float32)
         if i:
             ret[i, :, here] = acc.astype(jnp.bfloat16)
-            bk.append(
-                send(
-                    ret.at[i, :, here], back.at[z, :, here], bk_s.at[i, h], bk_r.at[i, h],
-                    (2 * plane[i] + core, t),
-                )
+            bk[(i, h)] = describe(
+                ret.at[i, :, here], back.at[z, :, here], bk_s.at[i, h], bk_r.at[i, h],
+                (2 * plane[i] + core, t),
             )
+            bk[(i, h)].start()
         else:
             back[z, :, here] = acc.astype(jnp.bfloat16)
 
@@ -539,68 +540,66 @@
     spread(0)
     dispatch(1)
     dispatch(2)
+    relay(0, 0)
+    relay(0, 1)
     dispatch(3)
-    relay(0)
+    spread(1)
     other(0)
-    spread(1)
+    corner(0)
+    relay(1, 0)
+    relay(1, 1)
     spread(2)
-    corner(0)
-    relay(1)
     widen(0, 0)
+    widen(0, 1)
     other(1)
-    widen(0, 1)
-    relay(2)
+    corner(1)
+    relay(2, 0)
+    relay(2, 1)
+    narrow(0, 0)
     spread(3)
-    narrow(0, 0)
-    corner(1)
+    widen(1, 0)
     other(2)
-    narrow(0, 1)
-    widen(1, 0)
-    combine(0, 0)
     widen(1, 1)
     corner(2)
     narrow(1, 0)
-    relay(3)
+    relay(3, 0)
+    relay(3, 1)
     widen(2, 0)
-    widen(2, 1)
     combine(1, 0)
     other(3)
+    widen(2, 1)
     narrow(2, 0)
-    combine(0, 1)
     corner(3)
     narrow(2, 1)
+    combine_on(1, 0)
     combine(2, 0)
     widen(3, 0)
-    combine_on(1, 0)
     combine(2, 1)
     widen(3, 1)
     narrow(3, 0)
     combine_on(2, 0)
-    narrow(3, 1)
+    narrow(1, 1)
     combine(3, 0)
     finish(1, 0)
-    narrow(1, 1)
+    narrow(3, 1)
+    combine_on(2, 1)
+    finish(2, 0)
     combine(3, 1)
+    combine_on(3, 0)
     combine(1, 1)
-    finish(2, 0)
-    combine_on(3, 0)
+    finish(2, 1)
     combine_on(3, 1)
-    combine_on(2, 1)
+    combine(0, 0)
+    finish(3, 0)
+    narrow(0, 1)
+    combine(0, 1)
     combine_on(1, 1)
-    finish(3, 0)
     finish(3, 1)
     combine_on(0, 0)
-    finish(2, 1)
+    combine_on(0, 1)
     finish(1, 1)
-    combine_on(0, 1)
     finish(0, 0)
     finish(0, 1)
-    for c in bk:
-        c.wait_recv()
-    routed = jnp.dot(
-        sel[1, :row_n, :], back[...].reshape(half, width), preferred_element_type=f32
-    )
-    out[...] = mid[...].astype(f32) + routed
     for c in sent:
         c.wait_send()
     for h in (0, 1):
@@ -611,6 +610,19 @@
     def _():
         for c in rims:
             c.wait_send()
+
+    for h in range(PIECES):
+        here = part_cols(0, h)
+        for i in range(1, GROUPS):
+            bk[(i, h)].wait_recv()
+        routed = jnp.dot(
+            sel[1, :row_n, :],
+            back[:, :, here].reshape(half, width // PIECES),
+            preferred_element_type=f32,
+        )
+        out[:, here] = mid[:, here].astype(f32) + routed
+    for c in bk.values():
+        c.wait_send()
 
 
 def group_layer(
@@ -682,8 +694,8 @@
             pltpu.VMEM((GROUPS, 2 * half, ext_width), bf),
             dma((GROUPS,)),
             dma((GROUPS,)),
-            dma((3, GROUPS)),
-            dma((3, GROUPS)),
+            dma((6, GROUPS)),
+            dma((6, GROUPS)),
             dma((4, GROUPS)),
             dma((4, GROUPS)),
             pltpu.VMEM((GROUPS, 2 * half, ff), bf),

time: 70.8 us -> 68.5 us (0.968)
  Pallas kernels: 69.9 us -> 67.6 us
    pallas_call x1, Pallas kernels: 69.9 us -> 67.6 us  [group_layer(): pl.pallas_call(group_kernel, out_shape=jax.ShapeDtypeStruct((row_n, width...]
where the time goes in v4:
time: 68.5 us; the launch traced here: 68.4 us
  Pallas kernels  67.6 us (99%)
  other arithmetic  0.73 us (1%)
    pallas_call x1, Pallas kernels, group_layer(): pl.pallas_call(group_kernel, out_shape=jax.ShapeDtypeStruct((row_n, width...  67.6 us

profile of v4, /device:TPU:0, one launch (start us, length us, event | category | flops | bytes accessed | tf_op | source)
XLA Modules:
  0.0 68.4 jit_solution(6201302191573130777)
XLA Ops:
  0.0 67.6 %shard_map.136 = f32[64,2048]{1,0:T(8,128)S(1)} custom-call(f32[8]{0:T(128)} %sink_hbm.1, bf16[256,512]{1,0:T(8,128)(2,1)} %q_hbm.1, bf16[256,256]{1,0:T(8,128)(2,1)} %k_hbm.1, bf16[256,256]{1,0:T(8,128)(2,1)} %v_hbm.1, f32[384,256]{1,0:T(8,128)} %constant.4.clone.row_hbm, f32[8,256]{1,0:T(8,128)} %constant.5.clone.base_hbm, bf16[64,2048]{1,0:T(8,128)(2,1)} %resid_hbm.1, ...), custom_call_target="tpu_custom_call" | custom-call | tf_op jit(solution)/shard_map/pallas_call | solution.py:656
  67.6 0.7 %convert_element_type.3 = bf16[64,2048]{1,0:T(8,128)(2,1)} convert(f32[64,2048]{1,0:T(8,128)S(1)} %shard_map.136) | non-fusion elementwise | flops 131072 | bytes 786432 | tf_op jit(solution)/shard_map/convert_element_type | solution.py:727

commit v5 on v4

--- a/solution.py
+++ b/solution.py
@@ -541,8 +541,8 @@
     dispatch(1)
     dispatch(2)
     relay(0, 0)
+    dispatch(3)
     relay(0, 1)
-    dispatch(3)
     spread(1)
     other(0)
     corner(0)
@@ -551,51 +551,51 @@
     spread(2)
     widen(0, 0)
     widen(0, 1)
+    corner(1)
     other(1)
-    corner(1)
     relay(2, 0)
     relay(2, 1)
+    spread(3)
     narrow(0, 0)
-    spread(3)
     widen(1, 0)
     other(2)
     widen(1, 1)
+    combine(0, 0)
     corner(2)
     narrow(1, 0)
     relay(3, 0)
     relay(3, 1)
     widen(2, 0)
+    widen(2, 1)
     combine(1, 0)
+    narrow(2, 0)
     other(3)
-    widen(2, 1)
-    narrow(2, 0)
+    narrow(2, 1)
     corner(3)
-    narrow(2, 1)
+    combine(2, 0)
     combine_on(1, 0)
-    combine(2, 0)
+    combine(2, 1)
     widen(3, 0)
-    combine(2, 1)
     widen(3, 1)
+    combine_on(2, 0)
     narrow(3, 0)
-    combine_on(2, 0)
-    narrow(1, 1)
-    combine(3, 0)
-    finish(1, 0)
     narrow(3, 1)
     combine_on(2, 1)
+    finish(1, 0)
+    combine(3, 0)
     finish(2, 0)
     combine(3, 1)
+    finish(2, 1)
     combine_on(3, 0)
+    narrow(1, 1)
     combine(1, 1)
-    finish(2, 1)
     combine_on(3, 1)
-    combine(0, 0)
     finish(3, 0)
     narrow(0, 1)
     combine(0, 1)
     combine_on(1, 1)
+    combine_on(0, 0)
     finish(3, 1)
-    combine_on(0, 0)
     combine_on(0, 1)
     finish(1, 1)
     finish(0, 0)

time: 68.5 us -> 69.5 us (1.015)
  Pallas kernels: 67.6 us -> 68.6 us
    pallas_call x1, Pallas kernels: 67.6 us -> 68.6 us  [group_layer(): pl.pallas_call(group_kernel, out_shape=jax.ShapeDtypeStruct((row_n, width...]
where the time goes in v5:
time: 69.5 us; the launch traced here: 69.3 us
  Pallas kernels  68.6 us (99%)
  other arithmetic  0.73 us (1%)
    pallas_call x1, Pallas kernels, group_layer(): pl.pallas_call(group_kernel, out_shape=jax.ShapeDtypeStruct((row_n, width...  68.6 us

profile of v5, /device:TPU:0, one launch (start us, length us, event | category | flops | bytes accessed | tf_op | source)
XLA Modules:
  0.0 69.3 jit_solution(2164059005591083700)
XLA Ops:
  0.0 68.6 %shard_map.136 = f32[64,2048]{1,0:T(8,128)S(1)} custom-call(f32[8]{0:T(128)} %sink_hbm.1, bf16[256,512]{1,0:T(8,128)(2,1)} %q_hbm.1, bf16[256,256]{1,0:T(8,128)(2,1)} %k_hbm.1, bf16[256,256]{1,0:T(8,128)(2,1)} %v_hbm.1, f32[384,256]{1,0:T(8,128)} %constant.4.clone.row_hbm, f32[8,256]{1,0:T(8,128)} %constant.5.clone.base_hbm, bf16[64,2048]{1,0:T(8,128)(2,1)} %resid_hbm.1, ...), custom_call_target="tpu_custom_call" | custom-call | tf_op jit(solution)/shard_map/pallas_call | solution.py:656
  68.6 0.7 %convert_element_type.3 = bf16[64,2048]{1,0:T(8,128)(2,1)} convert(f32[64,2048]{1,0:T(8,128)S(1)} %shard_map.136) | non-fusion elementwise | flops 131072 | bytes 786432 | tf_op jit(solution)/shard_map/convert_element_type | solution.py:727
